TPU v7x, 32 devices: a whole 2x2x4 slice. The times are simulated.
32 devices in a mesh: grp: 2 (over x), ep: 16 (over z, y, core).
Axes of the slice: x: 2, y: 2, z: 4, core: 2. Of those that a mesh axis runs over, the one named last changes fastest.
Arguments:
- tokens: bfloat16 [128, 2048], P(('grp', 'ep')), parts along dimension 0, may hold values from -6 to 6
- lengths: int32 [128], P(('grp', 'ep')), parts along dimension 0, may hold values from 128 to 1024, as said below
- cache_key: bfloat16 [128, 1024, 256], P(('grp', 'ep')), parts along dimension 0, may hold values from -6 to 6
- cache_value: bfloat16 [128, 1024, 256], P(('grp', 'ep')), parts along dimension 0, may hold values from -6 to 6
- routes: int32 [128, 2], P(('grp', 'ep')), parts along dimension 0, may hold values from 0 to 3, all different within a row
- route_logits: float32 [128, 2], P(('grp', 'ep')), parts along dimension 0, may hold values from -6 to 6
- mix_gain: float32 [2048], replicated, may hold values from 0.1 to 1.9
- query_gain: float32 [64], replicated, may hold values from 0.1 to 1.9
- key_gain: float32 [64], replicated, may hold values from 0.1 to 1.9
- head_bias: float32 [16], replicated, may hold values from -9 to -3.5
- w_query: bfloat16 [2048, 1024], P('ep'), may hold values from -0.125 to 0.125
- w_key: bfloat16 [2048, 256], P('ep'), may hold values from -0.125 to 0.125
- w_value: bfloat16 [2048, 256], P('ep'), may hold values from -0.125 to 0.125
- w_out: bfloat16 [1024, 2048], P(None, 'ep'), may hold values from -0.1875 to 0.1875
- ffn_gain: float32 [2048], replicated, may hold values from 0.1 to 1.9
- w_gate: bfloat16 [2048, 28672], P(None, 'ep'), may hold values from -0.125 to 0.125
- w_up: bfloat16 [2048, 28672], P(None, 'ep'), may hold values from -0.125 to 0.125
- w_down: bfloat16 [28672, 2048], P('ep'), may hold values from -0.0625 to 0.0625
Outputs:
- output: bfloat16 [128, 2048], P(('grp', 'ep')), parts along dimension 0
- new_key: bfloat16 [128, 256], P(('grp', 'ep')), parts along dimension 0
- new_value: bfloat16 [128, 256], P(('grp', 'ep')), parts along dimension 0
There are 2 independent parts, one for each index of `grp`. A program takes and returns all parts, laid end to end along the dimension named above; an argument that names none is the same for every part. Nothing has to cross between parts.
Inputs may be any that keep to these rules, and one draw needn't show every extreme that they name: `lengths`: some sequence has all 1024 positions live.
All inputs are finite; a program needn't handle non-finite values.
Results may differ from a plain program's by a relative error of at most 0.0085.
Values may be sent and summed in bfloat16 or wider, within the bound.
A program may use at most 128 MiB of HBM per device.

v0:
```python
import functools

import jax
import jax.numpy as jnp
from jax import lax
from jax.experimental import pallas as pl
from jax.experimental.pallas import tpu as pltpu
from jax.sharding import PartitionSpec as P

HEADS = 16
KV_HEADS = 4
HEAD_DIM = 64
FF = 7168
EXPERTS = 4


EPSILON = 1e-06


def rms_scaled(values, gain):
    return values * lax.rsqrt(jnp.mean(values * values, axis=-1, keepdims=True) + EPSILON) * gain


def route_weights(routes, route_logits):
    experts_iota = jnp.arange(EXPERTS, dtype=jnp.int32)[None, :]
    first_share = jax.nn.sigmoid(route_logits[:, 0:1] - route_logits[:, 1:2])
    second_share = jax.nn.sigmoid(route_logits[:, 1:2] - route_logits[:, 0:1])
    return jnp.where(routes[:, 0:1] == experts_iota, first_share, 0.0) + jnp.where(
        routes[:, 1:2] == experts_iota, second_share, 0.0
    )


def stick_attend(queries, lengths, cache_key, cache_value, query_gain, head_bias):
    batch_rows = queries.shape[0]
    cache_len = cache_key.shape[1]
    group_size = HEADS // KV_HEADS
    normed_query = rms_scaled(queries.reshape(batch_rows, HEADS, HEAD_DIM), query_gain).astype(
        jnp.bfloat16
    )
    normed_query = normed_query.reshape(batch_rows, KV_HEADS, group_size, HEAD_DIM)
    key_heads = cache_key.reshape(batch_rows, cache_len, KV_HEADS, HEAD_DIM)
    value_heads = cache_value.reshape(batch_rows, cache_len, KV_HEADS, HEAD_DIM)
    scores = jnp.einsum(
        "bkgd,blkd->bkgl", normed_query, key_heads, preferred_element_type=jnp.float32
    ) * HEAD_DIM ** (-0.5)
    scores = scores + head_bias.reshape(KV_HEADS, group_size)[None, :, :, None]
    live_mask = (
        jnp.arange(cache_len, dtype=jnp.int32)[None, None, None, :] < lengths[:, None, None, None]
    )
    remain = jnp.where(live_mask, jax.nn.log_sigmoid(-scores), 0.0)
    after_sum = lax.cumsum(remain, axis=3, reverse=True) - remain
    weights = jnp.where(live_mask, jnp.exp(jax.nn.log_sigmoid(scores) + after_sum), 0.0).astype(
        jnp.bfloat16
    )
    attended = jnp.einsum(
        "bkgl,blkd->bkgd", weights, value_heads, preferred_element_type=jnp.float32
    )
    return attended.reshape(batch_rows, HEADS * HEAD_DIM).astype(jnp.bfloat16)


def plain(
    tokens,
    lengths,
    cache_key,
    cache_value,
    routes,
    route_logits,
    mix_gain,
    query_gain,
    key_gain,
    head_bias,
    w_query,
    w_key,
    w_value,
    w_out,
    ffn_gain,
    w_gate,
    w_up,
    w_down,
):
    token_rows = tokens.shape[0]
    key_width = w_key.shape[1]
    as_float = tokens.astype(jnp.float32)
    normed = rms_scaled(as_float, mix_gain).astype(jnp.bfloat16)
    pieces = (
        lax.all_gather(w_query, "ep", axis=0, tiled=True),
        lax.all_gather(w_key, "ep", axis=0, tiled=True),
        lax.all_gather(w_value, "ep", axis=0, tiled=True),
    )
    queries, fresh_key, fresh_value = tuple(
        (jnp.dot(normed, weight, preferred_element_type=jnp.float32) for weight in pieces)
    )
    new_key = rms_scaled(fresh_key.reshape(token_rows, KV_HEADS, HEAD_DIM), key_gain)
    new_key = new_key.reshape(token_rows, key_width).astype(jnp.bfloat16)
    new_value = fresh_value.astype(jnp.bfloat16)
    attended = stick_attend(queries, lengths, cache_key, cache_value, query_gain, head_bias)
    mixed = as_float + jnp.dot(
        attended,
        lax.all_gather(w_out, "ep", axis=1, tiled=True),
        preferred_element_type=jnp.float32,
    )
    expert_in = rms_scaled(mixed, ffn_gain).astype(jnp.bfloat16)
    every_gate = lax.all_gather(route_weights(routes, route_logits), "ep", axis=0, tiled=True)
    ff_share = w_gate.shape[1]
    my_expert = lax.axis_index("ep") // (FF // ff_share)
    my_gate = lax.dynamic_slice_in_dim(every_gate, my_expert, 1, 1)
    input_rows = lax.all_gather(expert_in, "ep", axis=0, tiled=True)
    gate_value = jnp.dot(input_rows, w_gate, preferred_element_type=jnp.float32)
    up_value = jnp.dot(input_rows, w_up, preferred_element_type=jnp.float32)
    hidden = (jax.nn.silu(gate_value) * up_value * my_gate).astype(jnp.bfloat16)
    expert_sum = lax.psum_scatter(
        jnp.dot(hidden, w_down, preferred_element_type=jnp.float32),
        "ep",
        scatter_dimension=0,
        tiled=True,
    )
    return ((mixed + expert_sum).astype(jnp.bfloat16), new_key, new_value)


WEIGHT_PARTS = 2
DOWN_PARTS = 4
COLUMNS = 256


def dot(left, right):
    return jnp.dot(left, right, preferred_element_type=jnp.float32)


def iota(shape, dim):
    return lax.broadcasted_iota(jnp.int32, shape, dim)


def column(row):
    square = (row.shape[1], row.shape[1])
    return jnp.sum(
        jnp.where(iota(square, 0) == iota(square, 1), jnp.broadcast_to(row, square), 0.0),
        axis=1,
        keepdims=True,
    )


def finish(*refs):
    half = len(refs) // 2
    copies = [
        pltpu.make_async_copy(refs[i], refs[half + i], refs[-1].at[i]) for i in range(half)
    ]
    for copy in copies:
        copy.start()
    for copy in copies:
        copy.wait()


def fused(
    n,
    tokens_hbm,
    lengths_ref,
    ck_hbm,
    cv_hbm,
    routes_hbm,
    logits_hbm,
    mix_gain_hbm,
    query_gain_hbm,
    key_gain_hbm,
    head_bias_hbm,
    wq_hbm,
    wk_hbm,
    wv_hbm,
    wo_hbm,
    ffn_gain_hbm,
    wg_hbm,
    wu_hbm,
    wd_hbm,
    out_any,
    new_key_any,
    new_value_any,
    tokens_ref,
    routes_ref,
    logits_ref,
    mix_gain_ref,
    query_gain_ref,
    key_gain_ref,
    head_bias_ref,
    ffn_gain_ref,
    out_ref,
    new_key_ref,
    new_value_ref,
    wq,
    wk,
    wv,
    wo,
    ck,
    cv,
    wg,
    wu,
    wd,
    s1,
    r1,
    s2,
    p2,
    t2,
    r2,
    r3,
    r4,
    s5,
    p5,
    t5,
    r5,
    token_cols,
    aux_rows,
    attended_rows,
    expert_in,
    hidden,
    operand_sem,
    result_sem,
    small_sem,
    key_sem,
    value_sem,
    weight_sem,
    send_sem,
    recv_sem,
    block_sem,
    pair_send_sem,
    pair_sem,
):
    me = lax.axis_index("ep")
    rows, width = tokens_ref.shape
    all_rows = rows * n
    share = width // n
    q_width = wq.shape[1]
    k_width = wk.shape[1]
    cache_len = ck.shape[1]
    group_size = HEADS // KV_HEADS
    ff_share = wg.shape[1]
    my_expert = me // (FF // ff_share)

    barrier = pltpu.get_barrier_semaphore()
    peer_at = [me]
    for d in range(1, n):
        bit = d.bit_length() - 1
        flip = 2**bit * (1 - 2 * ((me // 2**bit) % 2))
        peer_at.append(peer_at[d - 2**bit] + flip)
    furthest_first = range(n - 1, 0, -1)
    core, chip = me % 2, me // 2
    for d in furthest_first:
        pl.semaphore_signal(
            barrier,
            inc=1,
            device_id={"ep": peer_at[d]},
            device_id_type=pl.DeviceIdType.MESH,
        )

    operands = [
        pltpu.make_async_copy(a, b, operand_sem.at[i])
        for i, (a, b) in enumerate(
            (
                (tokens_hbm, tokens_ref),
                (routes_hbm, routes_ref),
                (logits_hbm, logits_ref),
                (mix_gain_hbm, mix_gain_ref),
                (query_gain_hbm, query_gain_ref),
                (key_gain_hbm, key_gain_ref),
                (head_bias_hbm, head_bias_ref),
                (ffn_gain_hbm, ffn_gain_ref),
            )
        )
    ]
    for c in operands:
        c.start()

    small = [
        pltpu.make_async_copy(a, b, small_sem.at[i])
        for i, (a, b) in enumerate(((wq_hbm, wq), (wk_hbm, wk), (wv_hbm, wv), (wo_hbm, wo)))
    ]
    for c in small[:3]:
        c.start()
    keys = [pltpu.make_async_copy(ck_hbm.at[b], ck.at[b], key_sem.at[b]) for b in range(rows)]
    values = [pltpu.make_async_copy(cv_hbm.at[b], cv.at[b], value_sem.at[b]) for b in range(rows)]
    weights = []
    for which, (a, b) in enumerate(((wg_hbm, wg), (wu_hbm, wu), (wd_hbm, wd))):
        step = b.shape[0] // WEIGHT_PARTS
        for part in range(WEIGHT_PARTS):
            piece = pl.ds(part * step, step)
            weights.append(
                pltpu.make_async_copy(
                    a.at[piece], b.at[piece], weight_sem.at[which, part]
                )
            )

    results = [
        pltpu.make_async_copy(a, b, result_sem.at[i])
        for i, (a, b) in enumerate(
            ((out_ref, out_any), (new_key_ref, new_key_any), (new_value_ref, new_value_any))
        )
    ]
    for c in operands:
        c.wait()


    def send(stage, d, source, target, arrival=None):
        copy = pltpu.make_async_remote_copy(
            src_ref=source,
            dst_ref=target,
            send_sem=send_sem.at[stage],
            recv_sem=recv_sem.at[stage] if arrival is None else arrival,
            device_id={"ep": peer_at[d]},
            device_id_type=pl.DeviceIdType.MESH,
        )
        copy.start()

    def arrived(sem, blocks):
        pltpu.make_async_copy(blocks, blocks, sem).wait()

    others = pl.ds(0, n - 1)
    other_chips = pl.ds(0, n // 2 - 1)

    as_float = tokens_ref[...].astype(jnp.float32)
    scale = lax.rsqrt(jnp.mean(as_float * as_float, axis=1, keepdims=True) + EPSILON)
    lane = iota((rows, 128), 1)
    logit_gap = column(logits_ref[0:1] - logits_ref[1:2])
    chosen = [column(routes_ref[i : i + 1].astype(jnp.float32)) for i in range(2)]
    first_share = 1.0 / (1.0 + jnp.exp(-logit_gap))
    second_share = 1.0 / (1.0 + jnp.exp(logit_gap))
    expert_lane = (lane % EXPERTS).astype(jnp.float32)
    gates = jnp.where(chosen[0] == expert_lane, first_share, 0.0) + jnp.where(
        chosen[1] == expert_lane, second_share, 0.0
    )
    aux = jnp.where(lane < 3 * EXPERTS, gates, scale)
    high = aux.astype(jnp.bfloat16).astype(jnp.float32)
    middle = (aux - high).astype(jnp.bfloat16).astype(jnp.float32)
    low = aux - high - middle
    term = jnp.where(lane < 3 * EXPERTS, lane // EXPERTS, lane - 3 * EXPERTS)
    aux = jnp.where(term == 0, high, jnp.where(term == 1, middle, low))
    for peer in range(n):
        block = jnp.concatenate(
            [as_float[:, peer * share : (peer + 1) * share], aux], axis=0
        ).astype(jnp.bfloat16)
        s1[peer] = block
    pl.semaphore_wait(barrier, n - 1)
    for d in furthest_first:
        send(0, d, s1.at[peer_at[d]], r1.at[me])
    for c in keys + values + small[3:]:
        c.start()
    r1[me] = s1[me]
    for c in small[:3]:
        c.wait()
    arrived(recv_sem.at[0], r1.at[others])
    for c in weights:
        c.start()
    for peer in range(n):
        block = r1[peer].astype(jnp.float32)
        token_cols[peer * rows : (peer + 1) * rows, :] = block[:rows]
        aux_rows[peer * rows : (peer + 1) * rows, :] = block[rows:]
    aux = aux_rows[...]
    lane = iota(aux.shape, 1)
    row_scale = jnp.sum(
        jnp.where((lane >= 3 * EXPERTS) & (lane < 3 * EXPERTS + 3), aux, 0.0), axis=1, keepdims=True
    )
    my_gate = jnp.sum(
        jnp.where((lane < 3 * EXPERTS) & (lane % EXPERTS == my_expert), aux, 0.0),
        axis=1,
        keepdims=True,
    )
    my_gain = mix_gain_ref[:, pl.ds(pl.multiple_of(me * share, share), share)]
    normed = (token_cols[...] * row_scale * my_gain).astype(jnp.bfloat16)

    for weight, start in ((wq, 0), (wk, q_width), (wv, q_width + k_width)):
        partial = dot(normed, weight[...])
        for peer in range(n):
            s2[peer % 2, peer // 2, :, start : start + weight.shape[1]] = partial[
                peer * rows : (peer + 1) * rows
            ].astype(jnp.bfloat16)
    pair = pltpu.make_async_remote_copy(
        src_ref=s2.at[1 - core],
        dst_ref=p2,
        send_sem=pair_send_sem.at[DOWN_PARTS],
        recv_sem=pair_sem.at[DOWN_PARTS],
        device_id={"ep": peer_at[1]},
        device_id_type=pl.DeviceIdType.MESH,
    )
    pair.start()

    head_of_lane = iota((HEADS, q_width), 1) // HEAD_DIM
    own_lane = head_of_lane == iota((HEADS, q_width), 0)
    source_lane = iota((q_width, k_width), 0)
    target_lane = iota((q_width, k_width), 1)
    fold = jnp.where(
        (source_lane // (HEAD_DIM * group_size) == target_lane // HEAD_DIM)
        & (source_lane % HEAD_DIM == target_lane % HEAD_DIM),
        1.0,
        0.0,
    ).astype(jnp.bfloat16)
    later = jnp.where(
        iota((COLUMNS, COLUMNS), 0) > iota((COLUMNS, COLUMNS), 1), 1.0, 0.0
    ).astype(jnp.bfloat16)
    query_gain = jnp.concatenate([query_gain_ref[...]] * HEADS, axis=1)
    key_gain = jnp.concatenate([key_gain_ref[...]] * KV_HEADS, axis=1)

    pair.wait_recv()
    t2[...] = (s2[core].astype(jnp.float32) + p2[...].astype(jnp.float32)).astype(jnp.bfloat16)
    for d in range(n - 2, 0, -2):
        send(1, d, t2.at[peer_at[d] // 2], r2.at[chip])
    r2[chip] = t2[chip]
    arrived(recv_sem.at[1], r2.at[other_chips])
    total = r2[0].astype(jnp.float32)
    for peer in range(1, n // 2):
        total = total + r2[peer].astype(jnp.float32)
    queries = total[:, :q_width]
    fresh_key = total[:, q_width : q_width + k_width]
    new_value_ref[...] = total[:, q_width + k_width :].astype(jnp.bfloat16)
    squares = fresh_key * fresh_key
    key_lane = iota(squares.shape, 1) // HEAD_DIM
    key_scale = jnp.zeros_like(squares)
    for g in range(KV_HEADS):
        mean = jnp.sum(jnp.where(key_lane == g, squares, 0.0), axis=1, keepdims=True) / HEAD_DIM
        key_scale = jnp.where(key_lane == g, lax.rsqrt(mean + EPSILON), key_scale)
    new_key_ref[...] = (fresh_key * key_scale * key_gain).astype(jnp.bfloat16)

    for c in results[1:]:
        c.start()

    spread = []
    for b in range(rows):
        wide = jnp.where(own_lane, jnp.broadcast_to(queries[b : b + 1], own_lane.shape), 0.0)
        mean = jnp.sum(wide * wide, axis=1, keepdims=True) / HEAD_DIM
        spread.append((wide * lax.rsqrt(mean + EPSILON) * query_gain).astype(jnp.bfloat16))
    folded = dot(jnp.concatenate(spread, axis=0), fold).astype(jnp.bfloat16)
    blocks = cache_len // COLUMNS
    head_rows = rows * HEADS
    head_bias = jnp.concatenate([column(head_bias_ref[...])] * rows, axis=0)
    row_of = iota((head_rows, 1), 0) // HEADS
    lengths = jnp.zeros((head_rows, 1), jnp.int32)
    for b in range(rows):
        lengths = jnp.where(row_of == b, lengths_ref[b], lengths)
    live = iota((head_rows, cache_len), 1) < lengths
    for c in keys + values:
        c.wait()
    scores = jnp.concatenate(
        [
            lax.dot_general(
                folded[b * HEADS : (b + 1) * HEADS],
                ck[b],
                (((1,), (1,)), ((), ())),
                preferred_element_type=jnp.float32,
            )
            for b in range(rows)
        ],
        axis=0,
    )
    scores = scores * HEAD_DIM ** (-0.5) + head_bias
    tail_log = jnp.log1p(jnp.exp(-jnp.abs(scores)))
    remain = jnp.where(live, jnp.minimum(-scores, 0.0) - tail_log, 0.0)
    after = [None] * blocks
    carry = jnp.zeros((head_rows, 1), jnp.float32)
    for i in reversed(range(blocks)):
        block = remain[:, i * COLUMNS : (i + 1) * COLUMNS]
        high = block.astype(jnp.bfloat16)
        low = (block - high.astype(jnp.float32)).astype(jnp.bfloat16)
        after[i] = dot(high, later) + dot(low, later) + carry
        carry = carry + jnp.sum(block, axis=1, keepdims=True)
    after_sum = jnp.concatenate(after, axis=1)
    chance = jnp.exp(jnp.minimum(scores, 0.0) - tail_log + after_sum)
    weight = jnp.where(live, chance, 0.0).astype(jnp.bfloat16)
    mixed_heads = jnp.concatenate(
        [dot(weight[b * HEADS : (b + 1) * HEADS], cv[b]) for b in range(rows)], axis=0
    )
    own_group = (
        iota((head_rows, k_width), 1) // HEAD_DIM
        == iota((head_rows, k_width), 0) % HEADS // group_size
    )
    heads = jnp.where(own_group, mixed_heads, 0.0).astype(jnp.bfloat16)
    unfolded = lax.dot_general(
        heads,
        fold,
        (((1,), (1,)), ((), ())),
        preferred_element_type=jnp.float32,
    )
    attended = [
        jnp.sum(
            jnp.where(own_lane, unfolded[b * HEADS : (b + 1) * HEADS], 0.0), axis=0, keepdims=True
        )
        for b in range(rows)
    ]
    r3[me] = jnp.concatenate(attended, axis=0).astype(jnp.bfloat16)

    for d in furthest_first:
        send(2, d, r3.at[me], r3.at[me])
    small[3].wait()
    arrived(recv_sem.at[2], r3.at[others])
    for peer in range(n):
        attended_rows[peer * rows : (peer + 1) * rows, :] = r3[peer].astype(jnp.float32)
    mixed = token_cols[...] + dot(attended_rows[...].astype(jnp.bfloat16), wo[...])
    r4[me] = mixed.astype(jnp.bfloat16)

    for d in range(n - 2, 0, -2):
        send(3, d, r4.at[me], r4.at[me], block_sem.at[me])
    send(3, 1, r4.at[me], r4.at[me], block_sem.at[me])
    for d in range(2, n, 2):
        source = peer_at[d]
        arrived(block_sem.at[source], r4.at[source])
        send(3, 1, r4.at[source], r4.at[source], block_sem.at[source])
    for d in range(1, n, 2):
        source = peer_at[d]
        arrived(block_sem.at[source], r4.at[source])
    squares = jnp.zeros((all_rows, share), jnp.float32)
    for peer in range(n):
        block = r4[peer].astype(jnp.float32)
        squares = squares + block * block
    scale = lax.rsqrt(jnp.sum(squares, axis=1, keepdims=True) / width + EPSILON)
    pick = jnp.where(
        iota((8, all_rows), 1) == iota((8, all_rows), 0) + me * rows, 1.0, 0.0
    ).astype(jnp.bfloat16)
    own_mixed = []
    for peer in range(n):
        columns = slice(peer * share, (peer + 1) * share)
        block = r4[peer]
        own_mixed.append(dot(pick, block)[:rows])
        expert_in[:, columns] = (
            block.astype(jnp.float32) * scale * ffn_gain_ref[:, columns]
        ).astype(jnp.bfloat16)
    own_mixed = jnp.concatenate(own_mixed, axis=1)

    for c in weights[: 2 * WEIGHT_PARTS]:
        c.wait()

    def hidden_step(i, carry):
        columns = pl.ds(pl.multiple_of(i * COLUMNS, COLUMNS), COLUMNS)
        gate_value = dot(expert_in[...], wg[:, columns])
        up_value = dot(expert_in[...], wu[:, columns])
        silu = gate_value / (1.0 + jnp.exp(-gate_value))
        hidden[:, columns] = (silu * up_value * my_gate).astype(jnp.bfloat16)
        return carry

    lax.fori_loop(0, ff_share // COLUMNS, hidden_step, 0)

    for c in weights[2 * WEIGHT_PARTS :]:
        c.wait()

    step = width // DOWN_PARTS

    pairs = []

    def spread_sums(part):
        arrived(pair_sem.at[part], p5.at[part])
        both = s5[part, core].astype(jnp.float32) + p5[part].astype(jnp.float32)
        t5[part] = both.astype(jnp.bfloat16)
        for d in range(n - 2, 0, -2):
            send(4 + part, d, t5.at[part, peer_at[d] // 2], r5.at[part, chip])
        r5[part, chip] = t5[part, chip]

    for part in range(DOWN_PARTS):
        partial = dot(hidden[...], wd[:, part * step : (part + 1) * step])
        for peer in range(n):
            s5[part, peer % 2, peer // 2] = partial[peer * rows : (peer + 1) * rows].astype(
                jnp.bfloat16
            )
        pairs.append(
            pltpu.make_async_remote_copy(
                src_ref=s5.at[part, 1 - core],
                dst_ref=p5.at[part],
                send_sem=pair_send_sem.at[part],
                recv_sem=pair_sem.at[part],
                device_id={"ep": peer_at[1]},
                device_id_type=pl.DeviceIdType.MESH,
            )
        )
        pairs[-1].start()
        if part:
            spread_sums(part - 1)
    spread_sums(DOWN_PARTS - 1)
    for part in range(DOWN_PARTS):
        arrived(recv_sem.at[4 + part], r5.at[part, other_chips])
        total = own_mixed[:, part * step : (part + 1) * step]
        for peer in range(n // 2):
            total = total + r5[part, peer].astype(jnp.float32)
        out_ref[:, part * step : (part + 1) * step] = total.astype(jnp.bfloat16)
    results[0].start()
    for stage, blocks in enumerate((s1, None, r3, r4)):
        if blocks is not None:
            arrived(send_sem.at[stage], blocks.at[others])
    arrived(send_sem.at[1], t2.at[other_chips])
    pair.wait_send()
    for part in range(DOWN_PARTS):
        pairs[part].wait_send()
        arrived(send_sem.at[4 + part], t5.at[part, other_chips])
    for c in results:
        c.wait()


def local(
    n,
    tokens,
    lengths,
    cache_key,
    cache_value,
    routes,
    route_logits,
    mix_gain,
    query_gain,
    key_gain,
    head_bias,
    w_query,
    w_key,
    w_value,
    w_out,
    ffn_gain,
    w_gate,
    w_up,
    w_down,
):
    rows, width = tokens.shape
    all_rows = rows * n
    share = width // n
    q_width, k_width = w_query.shape[1], w_key.shape[1]
    wide = q_width + k_width + w_value.shape[1]
    stages = 4 + DOWN_PARTS
    anywhere = pl.BlockSpec(memory_space=pl.ANY)
    smem = pl.BlockSpec(memory_space=pltpu.SMEM)
    bf16, f32 = jnp.bfloat16, jnp.float32

    def like(array):
        return pltpu.VMEM(array.shape, array.dtype)

    flops = 2 * all_rows * 3 * w_gate.shape[0] * w_gate.shape[1]
    shapes = ((rows, width), (rows, k_width), (rows, w_value.shape[1]))
    results = pl.pallas_call(
        functools.partial(fused, n),
        out_shape=tuple(pltpu.VMEM(shape, bf16) for shape in shapes),
        in_specs=[anywhere, smem] + [anywhere] * 16,
        out_specs=(anywhere,) * 3,
        scratch_shapes=[
            like(tokens),
            pltpu.VMEM(routes.shape[::-1], routes.dtype),
            pltpu.VMEM(route_logits.shape[::-1], f32),
            pltpu.VMEM((1, width), f32),
            pltpu.VMEM((1, HEAD_DIM), f32),
            pltpu.VMEM((1, HEAD_DIM), f32),
            pltpu.VMEM((1, HEADS), f32),
            pltpu.VMEM((1, width), f32),
            *(pltpu.VMEM(shape, bf16) for shape in shapes),
            like(w_query),
            like(w_key),
            like(w_value),
            like(w_out),
            like(cache_key),
            like(cache_value),
            like(w_gate),
            like(w_up),
            like(w_down),
            pltpu.VMEM((n, 2 * rows, share), bf16),
            pltpu.VMEM((n, 2 * rows, share), bf16),
            pltpu.VMEM((2, n // 2, rows, wide), bf16),
            pltpu.VMEM((n // 2, rows, wide), bf16),
            pltpu.VMEM((n // 2, rows, wide), bf16),
            pltpu.VMEM((n // 2, rows, wide), bf16),
            pltpu.VMEM((n, rows, q_width), bf16),
            pltpu.VMEM((n, all_rows, share), bf16),
            pltpu.VMEM((DOWN_PARTS, 2, n // 2, rows, width // DOWN_PARTS), bf16),
            pltpu.VMEM((DOWN_PARTS, n // 2, rows, width // DOWN_PARTS), bf16),
            pltpu.VMEM((DOWN_PARTS, n // 2, rows, width // DOWN_PARTS), bf16),
            pltpu.VMEM((DOWN_PARTS, n // 2, rows, width // DOWN_PARTS), bf16),
            pltpu.VMEM((all_rows, share), f32),
            pltpu.VMEM((all_rows, share), f32),
            pltpu.VMEM((all_rows, q_width), f32),
            pltpu.VMEM((all_rows, width), bf16),
            pltpu.VMEM((all_rows, w_gate.shape[1]), bf16),
            pltpu.SemaphoreType.DMA((8,)),
            pltpu.SemaphoreType.DMA((3,)),
            pltpu.SemaphoreType.DMA((4,)),
            pltpu.SemaphoreType.DMA((rows,)),
            pltpu.SemaphoreType.DMA((rows,)),
            pltpu.SemaphoreType.DMA((3, WEIGHT_PARTS)),
            pltpu.SemaphoreType.DMA((stages,)),
            pltpu.SemaphoreType.DMA((stages,)),
            pltpu.SemaphoreType.DMA((n,)),
            pltpu.SemaphoreType.DMA((DOWN_PARTS + 1,)),
            pltpu.SemaphoreType.DMA((DOWN_PARTS + 1,)),
        ],
        compiler_params=pltpu.CompilerParams(
            collective_id=0, has_side_effects=True, vmem_limit_bytes=60 * 1024 * 1024
        ),
        cost_estimate=pl.CostEstimate(flops=flops, bytes_accessed=flops // all_rows, transcendentals=0),
    )(
        tokens,
        lengths,
        cache_key,
        cache_value,
        routes.T,
        route_logits.T,
        mix_gain.reshape(1, -1),
        query_gain.reshape(1, -1),
        key_gain.reshape(1, -1),
        head_bias.reshape(1, -1),
        w_query,
        w_key,
        w_value,
        w_out,
        ffn_gain.reshape(1, -1),
        w_gate,
        w_up,
        w_down,
    )
    return pl.pallas_call(
        finish,
        out_shape=tuple(jax.ShapeDtypeStruct(shape, bf16) for shape in shapes),
        in_specs=[anywhere] * len(shapes),
        out_specs=(anywhere,) * len(shapes),
        scratch_shapes=[pltpu.SemaphoreType.DMA((len(shapes),))],
    )(*(pltpu.with_memory_space_constraint(result, pltpu.VMEM) for result in results))


def solution(mesh):
    n = mesh.shape["ep"]

    def body(*arrays):
        tokens, w_gate = arrays[0], arrays[15]
        share = tokens.shape[1] // n
        if share == 128 and n & (n - 1) == 0 and w_gate.shape[1] % COLUMNS == 0:
            return local(n, *arrays)
        return plain(*arrays)

    return jax.shard_map(
        body,
        mesh=mesh,
        in_specs=(
            P(("grp", "ep"), None),
            P(("grp", "ep")),
            P(("grp", "ep"), None, None),
            P(("grp", "ep"), None, None),
            P(("grp", "ep"), None),
            P(("grp", "ep"), None),
            P(),
            P(),
            P(),
            P(),
            P("ep", None),
            P("ep", None),
            P("ep", None),
            P(None, "ep"),
            P(),
            P(None, "ep"),
            P(None, "ep"),
            P("ep", None),
        ),
        out_specs=(P(("grp", "ep"), None), P(("grp", "ep"), None), P(("grp", "ep"), None)),
        check_vma=False,
    )
```

profile of v0, /device:TPU:0, one launch (start us, length us, event | category | flops | bytes accessed | tf_op | source)
XLA Modules:
  0.0 41.5 jit_solution(15267929637288289584)
XLA Ops:
  0.6 40.2 %shard_map.193 = (bf16[4,2048]{1,0:T(4,128)(2,1)S(1)}, bf16[4,256]{1,0:T(4,128)(2,1)S(1)}, bf16[4,256]{1,0:T(4,128)(2,1)S(1)}) custom-call(bf16[4,2048]{1,0:T(4,128)(2,1)} %tokens_hbm.1, s32[4]{0:T(128)} %lengths_ref.1, bf16[4,1024,256]{2,1,0:T(8,128)(2,1)} %ck_hbm.1, bf16[4,1024,256]{2,1,0:T(8,128)(2,1)} %cv_hbm.1, s32[2,4]{1,0:T(2,128)} %bitcast.9, ...), custom_call_target="tpu_custom_call" | custom-call | flops 1409286144 | bytes 22020096 | tf_op jit(solution)/shard_map/pallas_call | solution.py:625
  40.8 0.6 %shard_map.194 = (bf16[4,2048]{1,0:T(4,128)(2,1)}, bf16[4,256]{1,0:T(4,128)(2,1)}, bf16[4,256]{1,0:T(4,128)(2,1)}) custom-call(bf16[4,2048]{1,0:T(4,128)(2,1)S(1)} %get-tuple-element.6.refs_0_, bf16[4,256]{1,0:T(4,128)(2,1)S(1)} %get-tuple-element.7.refs_1_, bf16[4,256]{1,0:T(4,128)(2,1)S(1)} %get-tuple-element.8.refs_2_), custom_call_target="tpu_custom_call" | custom-call | tf_op jit(solution)/shard_map/pallas_call | solution.py:702
where the time goes:
time: 41.7 us; the launch traced here: 41.5 us
  Pallas kernels  40.8 us (98%)
  between operations  0.65 us (2%)
    pallas_call x1, Pallas kernels, local(): pl.pallas_call(functools.partial(fused, n), out_shape=tuple((pltpu.VMEM(s...  40.2 us

commit v1 on v0

--- a/solution.py
+++ b/solution.py
@@ -153,7 +153,7 @@
 def fused(
     n,
     tokens_hbm,
-    lengths_ref,
+    lengths_hbm,
     ck_hbm,
     cv_hbm,
     routes_hbm,
@@ -174,6 +174,7 @@
     new_key_any,
     new_value_any,
     tokens_ref,
+    lengths_ref,
     routes_ref,
     logits_ref,
     mix_gain_ref,
@@ -184,9 +185,7 @@
     out_ref,
     new_key_ref,
     new_value_ref,
-    wq,
-    wk,
-    wv,
+    wqkv,
     wo,
     ck,
     cv,
@@ -196,56 +195,63 @@
     s1,
     r1,
     s2,
-    p2,
-    t2,
     r2,
     r3,
     r4,
     s5,
     p5,
+    own5,
     t5,
     r5,
+    gates_all,
     token_cols,
     aux_rows,
     attended_rows,
-    expert_in,
+    own_mixed,
+    gate_acc,
+    up_acc,
     hidden,
     operand_sem,
     result_sem,
     small_sem,
-    key_sem,
-    value_sem,
+    cache_sem,
     weight_sem,
     send_sem,
     recv_sem,
-    block_sem,
-    pair_send_sem,
+    direct_sem,
+    relay_sem,
     pair_sem,
+    spread_sem,
+    twin_sem,
 ):
     me = lax.axis_index("ep")
+    core, chip = me % 2, me // 2
+    chips = n // 2
+    sibling = me + 1 - 2 * core
     rows, width = tokens_ref.shape
+    half_rows = rows * chips
     all_rows = rows * n
     share = width // n
-    q_width = wq.shape[1]
-    k_width = wk.shape[1]
+    chip_share = width // chips
+    q_width, k_width = wq_hbm.shape[1], wk_hbm.shape[1]
     cache_len = ck.shape[1]
     group_size = HEADS // KV_HEADS
     ff_share = wg.shape[1]
     my_expert = me // (FF // ff_share)
 
     barrier = pltpu.get_barrier_semaphore()
-    peer_at = [me]
-    for d in range(1, n):
-        bit = d.bit_length() - 1
-        flip = 2**bit * (1 - 2 * ((me // 2**bit) % 2))
-        peer_at.append(peer_at[d - 2**bit] + flip)
-    furthest_first = range(n - 1, 0, -1)
-    core, chip = me % 2, me // 2
-    for d in furthest_first:
+    chip_at = [chip]
+    for k in range(1, chips):
+        bit = k.bit_length() - 1
+        flip = 2**bit * (1 - 2 * ((chip // 2**bit) % 2))
+        chip_at.append(chip_at[k - 2**bit] + flip)
+    peer_at = [2 * c + core for c in chip_at]
+    furthest_first = range(chips - 1, 0, -1)
+    for device in [peer_at[k] for k in furthest_first] + [sibling]:
         pl.semaphore_signal(
             barrier,
             inc=1,
-            device_id={"ep": peer_at[d]},
+            device_id={"ep": device},
             device_id_type=pl.DeviceIdType.MESH,
         )
 
@@ -261,30 +267,35 @@
                 (key_gain_hbm, key_gain_ref),
                 (head_bias_hbm, head_bias_ref),
                 (ffn_gain_hbm, ffn_gain_ref),
+                (lengths_hbm, lengths_ref),
             )
         )
     ]
     for c in operands:
         c.start()
 
+    my_rows = pl.ds(pl.multiple_of(core * share, share), share)
     small = [
         pltpu.make_async_copy(a, b, small_sem.at[i])
-        for i, (a, b) in enumerate(((wq_hbm, wq), (wk_hbm, wk), (wv_hbm, wv), (wo_hbm, wo)))
+        for i, (a, b) in enumerate(
+            (
+                (wq_hbm, wqkv.at[my_rows, 0:q_width]),
+                (wk_hbm, wqkv.at[my_rows, q_width : q_width + k_width]),
+                (wv_hbm, wqkv.at[my_rows, q_width + k_width :]),
+                (wo_hbm, wo.at[core]),
+            )
+        )
     ]
-    for c in small[:3]:
+    for c in small:
         c.start()
-    keys = [pltpu.make_async_copy(ck_hbm.at[b], ck.at[b], key_sem.at[b]) for b in range(rows)]
-    values = [pltpu.make_async_copy(cv_hbm.at[b], cv.at[b], value_sem.at[b]) for b in range(rows)]
+    caches = [pltpu.make_async_copy(ck_hbm.at[b], ck.at[b], cache_sem.at[0]) for b in range(rows)]
+    caches += [pltpu.make_async_copy(cv_hbm.at[b], cv.at[b], cache_sem.at[1]) for b in range(rows)]
     weights = []
     for which, (a, b) in enumerate(((wg_hbm, wg), (wu_hbm, wu), (wd_hbm, wd))):
         step = b.shape[0] // WEIGHT_PARTS
         for part in range(WEIGHT_PARTS):
             piece = pl.ds(part * step, step)
-            weights.append(
-                pltpu.make_async_copy(
-                    a.at[piece], b.at[piece], weight_sem.at[which, part]
-                )
-            )
+            weights.append(pltpu.make_async_copy(a.at[piece], b.at[piece], weight_sem.at[which]))
 
     results = [
         pltpu.make_async_copy(a, b, result_sem.at[i])
@@ -295,23 +306,20 @@
     for c in operands:
         c.wait()
 
-
-    def send(stage, d, source, target, arrival=None):
-        copy = pltpu.make_async_remote_copy(
+    def send(stage, device, source, target, arrival):
+        pltpu.make_async_remote_copy(
             src_ref=source,
             dst_ref=target,
             send_sem=send_sem.at[stage],
-            recv_sem=recv_sem.at[stage] if arrival is None else arrival,
-            device_id={"ep": peer_at[d]},
+            recv_sem=arrival,
+            device_id={"ep": device},
             device_id_type=pl.DeviceIdType.MESH,
-        )
-        copy.start()
+        ).start()
 
     def arrived(sem, blocks):
         pltpu.make_async_copy(blocks, blocks, sem).wait()
 
-    others = pl.ds(0, n - 1)
-    other_chips = pl.ds(0, n // 2 - 1)
+    others = pl.ds(0, chips - 1)
 
     as_float = tokens_ref[...].astype(jnp.float32)
     scale = lax.rsqrt(jnp.mean(as_float * as_float, axis=1, keepdims=True) + EPSILON)
@@ -330,54 +338,51 @@
     low = aux - high - middle
     term = jnp.where(lane < 3 * EXPERTS, lane // EXPERTS, lane - 3 * EXPERTS)
     aux = jnp.where(term == 0, high, jnp.where(term == 1, middle, low))
-    for peer in range(n):
-        block = jnp.concatenate(
-            [as_float[:, peer * share : (peer + 1) * share], aux], axis=0
+    aux = jnp.concatenate([aux] * (chip_share // 128), axis=1)
+    for p in range(chips):
+        s1[p] = jnp.concatenate(
+            [as_float[:, p * chip_share : (p + 1) * chip_share], aux], axis=0
         ).astype(jnp.bfloat16)
-        s1[peer] = block
-    pl.semaphore_wait(barrier, n - 1)
-    for d in furthest_first:
-        send(0, d, s1.at[peer_at[d]], r1.at[me])
-    for c in keys + values + small[3:]:
-        c.start()
-    r1[me] = s1[me]
+    pl.semaphore_wait(barrier, chips)
+    for k in furthest_first:
+        send(0, peer_at[k], s1.at[chip_at[k]], r1.at[chip], recv_sem.at[0])
     for c in small[:3]:
         c.wait()
+    send(4, sibling, wqkv.at[my_rows], wqkv.at[my_rows], twin_sem.at[0])
+    small[3].wait()
+    send(5, sibling, wo.at[core], wo.at[core], twin_sem.at[1])
+    for c in caches:
+        c.start()
+    r1[chip] = s1[chip]
     arrived(recv_sem.at[0], r1.at[others])
     for c in weights:
         c.start()
-    for peer in range(n):
-        block = r1[peer].astype(jnp.float32)
-        token_cols[peer * rows : (peer + 1) * rows, :] = block[:rows]
-        aux_rows[peer * rows : (peer + 1) * rows, :] = block[rows:]
+    for p in range(chips):
+        block = r1[p].astype(jnp.float32)
+        token_cols[p * rows : (p + 1) * rows, :] = block[:rows]
+        aux_rows[p * rows : (p + 1) * rows, :] = block[rows:, :128]
     aux = aux_rows[...]
     lane = iota(aux.shape, 1)
     row_scale = jnp.sum(
         jnp.where((lane >= 3 * EXPERTS) & (lane < 3 * EXPERTS + 3), aux, 0.0), axis=1, keepdims=True
     )
+    my_gain = mix_gain_ref[:, pl.ds(pl.multiple_of(chip * chip_share, chip_share), chip_share)]
+    normed = (token_cols[...] * row_scale * my_gain).astype(jnp.bfloat16)
+    arrived(twin_sem.at[0], wqkv.at[my_rows])
+
+    partial = dot(normed, wqkv[...])
+    for p in range(chips):
+        s2[p] = partial[p * rows : (p + 1) * rows].astype(jnp.bfloat16)
+    for k in furthest_first:
+        send(1, peer_at[k], s2.at[chip_at[k]], r2.at[chip], recv_sem.at[1])
+    r2[chip] = s2[chip]
     my_gate = jnp.sum(
         jnp.where((lane < 3 * EXPERTS) & (lane % EXPERTS == my_expert), aux, 0.0),
         axis=1,
         keepdims=True,
     )
-    my_gain = mix_gain_ref[:, pl.ds(pl.multiple_of(me * share, share), share)]
-    normed = (token_cols[...] * row_scale * my_gain).astype(jnp.bfloat16)
-
-    for weight, start in ((wq, 0), (wk, q_width), (wv, q_width + k_width)):
-        partial = dot(normed, weight[...])
-        for peer in range(n):
-            s2[peer % 2, peer // 2, :, start : start + weight.shape[1]] = partial[
-                peer * rows : (peer + 1) * rows
-            ].astype(jnp.bfloat16)
-    pair = pltpu.make_async_remote_copy(
-        src_ref=s2.at[1 - core],
-        dst_ref=p2,
-        send_sem=pair_send_sem.at[DOWN_PARTS],
-        recv_sem=pair_sem.at[DOWN_PARTS],
-        device_id={"ep": peer_at[1]},
-        device_id_type=pl.DeviceIdType.MESH,
-    )
-    pair.start()
+    gates_all[core] = jnp.broadcast_to(my_gate, aux.shape)
+    send(6, sibling, gates_all.at[core], gates_all.at[core], twin_sem.at[2])
 
     head_of_lane = iota((HEADS, q_width), 1) // HEAD_DIM
     own_lane = head_of_lane == iota((HEADS, q_width), 0)
@@ -394,46 +399,28 @@
     ).astype(jnp.bfloat16)
     query_gain = jnp.concatenate([query_gain_ref[...]] * HEADS, axis=1)
     key_gain = jnp.concatenate([key_gain_ref[...]] * KV_HEADS, axis=1)
-
-    pair.wait_recv()
-    t2[...] = (s2[core].astype(jnp.float32) + p2[...].astype(jnp.float32)).astype(jnp.bfloat16)
-    for d in range(n - 2, 0, -2):
-        send(1, d, t2.at[peer_at[d] // 2], r2.at[chip])
-    r2[chip] = t2[chip]
-    arrived(recv_sem.at[1], r2.at[other_chips])
+    blocks = cache_len // COLUMNS
+    head_rows = rows * HEADS
+    head_bias = jnp.concatenate([column(head_bias_ref[...])] * rows, axis=0)
+    row_of = iota((head_rows, 1), 0) // HEADS
+    lengths = jnp.zeros((head_rows, 1), jnp.int32)
+    for b in range(rows):
+        lengths = jnp.where(row_of == b, lengths_ref[:, b : b + 1], lengths)
+    live = iota((head_rows, cache_len), 1) < lengths
+    arrived(cache_sem.at[0], ck)
+    arrived(cache_sem.at[1], cv)
+
+    arrived(recv_sem.at[1], r2.at[others])
     total = r2[0].astype(jnp.float32)
-    for peer in range(1, n // 2):
-        total = total + r2[peer].astype(jnp.float32)
+    for p in range(1, chips):
+        total = total + r2[p].astype(jnp.float32)
     queries = total[:, :q_width]
-    fresh_key = total[:, q_width : q_width + k_width]
-    new_value_ref[...] = total[:, q_width + k_width :].astype(jnp.bfloat16)
-    squares = fresh_key * fresh_key
-    key_lane = iota(squares.shape, 1) // HEAD_DIM
-    key_scale = jnp.zeros_like(squares)
-    for g in range(KV_HEADS):
-        mean = jnp.sum(jnp.where(key_lane == g, squares, 0.0), axis=1, keepdims=True) / HEAD_DIM
-        key_scale = jnp.where(key_lane == g, lax.rsqrt(mean + EPSILON), key_scale)
-    new_key_ref[...] = (fresh_key * key_scale * key_gain).astype(jnp.bfloat16)
-
-    for c in results[1:]:
-        c.start()
-
     spread = []
     for b in range(rows):
         wide = jnp.where(own_lane, jnp.broadcast_to(queries[b : b + 1], own_lane.shape), 0.0)
         mean = jnp.sum(wide * wide, axis=1, keepdims=True) / HEAD_DIM
         spread.append((wide * lax.rsqrt(mean + EPSILON) * query_gain).astype(jnp.bfloat16))
     folded = dot(jnp.concatenate(spread, axis=0), fold).astype(jnp.bfloat16)
-    blocks = cache_len // COLUMNS
-    head_rows = rows * HEADS
-    head_bias = jnp.concatenate([column(head_bias_ref[...])] * rows, axis=0)
-    row_of = iota((head_rows, 1), 0) // HEADS
-    lengths = jnp.zeros((head_rows, 1), jnp.int32)
-    for b in range(rows):
-        lengths = jnp.where(row_of == b, lengths_ref[b], lengths)
-    live = iota((head_rows, cache_len), 1) < lengths
-    for c in keys + values:
-        c.wait()
     scores = jnp.concatenate(
         [
             lax.dot_general(
@@ -480,108 +467,117 @@
         )
         for b in range(rows)
     ]
-    r3[me] = jnp.concatenate(attended, axis=0).astype(jnp.bfloat16)
-
-    for d in furthest_first:
-        send(2, d, r3.at[me], r3.at[me])
-    small[3].wait()
+    r3[chip] = jnp.concatenate(attended, axis=0).astype(jnp.bfloat16)
+
+    for k in furthest_first:
+        send(2, peer_at[k], r3.at[chip], r3.at[chip], recv_sem.at[2])
+
+    fresh_key = total[:, q_width : q_width + k_width]
+    new_value_ref[...] = total[:, q_width + k_width :].astype(jnp.bfloat16)
+    squares = fresh_key * fresh_key
+    key_lane = iota(squares.shape, 1) // HEAD_DIM
+    key_scale = jnp.zeros_like(squares)
+    for g in range(KV_HEADS):
+        mean = jnp.sum(jnp.where(key_lane == g, squares, 0.0), axis=1, keepdims=True) / HEAD_DIM
+        key_scale = jnp.where(key_lane == g, lax.rsqrt(mean + EPSILON), key_scale)
+    new_key_ref[...] = (fresh_key * key_scale * key_gain).astype(jnp.bfloat16)
+    for c in results[1:]:
+        c.start()
+    arrived(twin_sem.at[1], wo.at[core])
+    arrived(twin_sem.at[2], gates_all.at[core])
+
     arrived(recv_sem.at[2], r3.at[others])
-    for peer in range(n):
-        attended_rows[peer * rows : (peer + 1) * rows, :] = r3[peer].astype(jnp.float32)
-    mixed = token_cols[...] + dot(attended_rows[...].astype(jnp.bfloat16), wo[...])
-    r4[me] = mixed.astype(jnp.bfloat16)
-
-    for d in range(n - 2, 0, -2):
-        send(3, d, r4.at[me], r4.at[me], block_sem.at[me])
-    send(3, 1, r4.at[me], r4.at[me], block_sem.at[me])
-    for d in range(2, n, 2):
-        source = peer_at[d]
-        arrived(block_sem.at[source], r4.at[source])
-        send(3, 1, r4.at[source], r4.at[source], block_sem.at[source])
-    for d in range(1, n, 2):
-        source = peer_at[d]
-        arrived(block_sem.at[source], r4.at[source])
-    squares = jnp.zeros((all_rows, share), jnp.float32)
-    for peer in range(n):
-        block = r4[peer].astype(jnp.float32)
+    for p in range(chips):
+        attended_rows[p * rows : (p + 1) * rows, :] = r3[p].astype(jnp.float32)
+    attended_all = attended_rows[...].astype(jnp.bfloat16)
+    for h in range(2):
+        columns = slice(h * share, (h + 1) * share)
+        mixed = token_cols[:, columns] + dot(attended_all, wo[h])
+        r4[chip, core, :, columns] = mixed.astype(jnp.bfloat16)
+
+    mine = r4.at[chip, core]
+    for k in furthest_first:
+        send(3, peer_at[k], mine, mine, direct_sem.at[k])
+    send(7, sibling, mine, mine, relay_sem.at[0])
+    pick = jnp.where(
+        iota((8, half_rows), 1) == iota((8, half_rows), 0) + chip * rows, 1.0, 0.0
+    ).astype(jnp.bfloat16)
+    squares = jnp.zeros((all_rows, chip_share), jnp.float32)
+    gate_column = gates_all[...].reshape(all_rows, 128)[:, :1]
+    for which, b in enumerate((wg, wu, wd)):
+        arrived(weight_sem.at[which], b)
+
+    def chunk(k, squares):
+        source = chip_at[k]
+        columns = pl.ds(pl.multiple_of(source * chip_share, chip_share), chip_share)
+        arrived(relay_sem.at[k], r4.at[source, core])
+        own_mixed[:, columns] = dot(pick, r4[source, core])[:rows]
+        block = r4[source].reshape(all_rows, chip_share).astype(jnp.float32)
         squares = squares + block * block
-    scale = lax.rsqrt(jnp.sum(squares, axis=1, keepdims=True) / width + EPSILON)
-    pick = jnp.where(
-        iota((8, all_rows), 1) == iota((8, all_rows), 0) + me * rows, 1.0, 0.0
-    ).astype(jnp.bfloat16)
-    own_mixed = []
-    for peer in range(n):
-        columns = slice(peer * share, (peer + 1) * share)
-        block = r4[peer]
-        own_mixed.append(dot(pick, block)[:rows])
-        expert_in[:, columns] = (
-            block.astype(jnp.float32) * scale * ffn_gain_ref[:, columns]
-        ).astype(jnp.bfloat16)
-    own_mixed = jnp.concatenate(own_mixed, axis=1)
-
-    for c in weights[: 2 * WEIGHT_PARTS]:
-        c.wait()
-
-    def hidden_step(i, carry):
-        columns = pl.ds(pl.multiple_of(i * COLUMNS, COLUMNS), COLUMNS)
-        gate_value = dot(expert_in[...], wg[:, columns])
-        up_value = dot(expert_in[...], wu[:, columns])
-        silu = gate_value / (1.0 + jnp.exp(-gate_value))
-        hidden[:, columns] = (silu * up_value * my_gate).astype(jnp.bfloat16)
-        return carry
-
-    lax.fori_loop(0, ff_share // COLUMNS, hidden_step, 0)
-
-    for c in weights[2 * WEIGHT_PARTS :]:
-        c.wait()
+        entry = (block * ffn_gain_ref[:, columns]).astype(jnp.bfloat16)
+        if k == chips - 1:
+            scale = lax.rsqrt(jnp.sum(squares, axis=1, keepdims=True) / width + EPSILON)
+        for i in range(ff_share // COLUMNS):
+            inner = slice(i * COLUMNS, (i + 1) * COLUMNS)
+            gate_value = dot(entry, wg[columns, inner])
+            up_value = dot(entry, wu[columns, inner])
+            if k:
+                gate_value = gate_value + gate_acc[:, inner]
+                up_value = up_value + up_acc[:, inner]
+            if k == chips - 1:
+                gate_value = gate_value * scale
+                silu = gate_value / (1.0 + jnp.exp(-gate_value))
+                hidden[:, inner] = (silu * (up_value * scale) * gate_column).astype(jnp.bfloat16)
+            else:
+                gate_acc[:, inner] = gate_value
+                up_acc[:, inner] = up_value
+        return squares
+
+    for k in range(1, chips):
+        block = r4.at[chip_at[k], core]
+        arrived(direct_sem.at[k], block)
+        send(7, sibling, block, block, relay_sem.at[k])
+        squares = chunk(k - 1, squares)
+    squares = chunk(chips - 1, squares)
 
     step = width // DOWN_PARTS
-
-    pairs = []
 
     def spread_sums(part):
         arrived(pair_sem.at[part], p5.at[part])
-        both = s5[part, core].astype(jnp.float32) + p5[part].astype(jnp.float32)
-        t5[part] = both.astype(jnp.bfloat16)
-        for d in range(n - 2, 0, -2):
-            send(4 + part, d, t5.at[part, peer_at[d] // 2], r5.at[part, chip])
+        both = own5[part] + p5[part].astype(jnp.float32)
+        for p in range(chips):
+            t5[part, p] = both[p * rows : (p + 1) * rows].astype(jnp.bfloat16)
+        for k in furthest_first:
+            send(9, peer_at[k], t5.at[part, chip_at[k]], r5.at[part, chip], spread_sem.at[part])
         r5[part, chip] = t5[part, chip]
 
     for part in range(DOWN_PARTS):
         partial = dot(hidden[...], wd[:, part * step : (part + 1) * step])
-        for peer in range(n):
-            s5[part, peer % 2, peer // 2] = partial[peer * rows : (peer + 1) * rows].astype(
-                jnp.bfloat16
-            )
-        pairs.append(
-            pltpu.make_async_remote_copy(
-                src_ref=s5.at[part, 1 - core],
-                dst_ref=p5.at[part],
-                send_sem=pair_send_sem.at[part],
-                recv_sem=pair_sem.at[part],
-                device_id={"ep": peer_at[1]},
-                device_id_type=pl.DeviceIdType.MESH,
-            )
-        )
-        pairs[-1].start()
-        if part:
-            spread_sums(part - 1)
+        lower, upper = partial[:half_rows], partial[half_rows:]
+        own5[part] = jnp.where(core == 0, lower, upper)
+        s5[part] = jnp.where(core == 0, upper, lower).astype(jnp.bfloat16)
+        send(8, sibling, s5.at[part], p5.at[part], pair_sem.at[part])
+        if part > 1:
+            spread_sums(part - 2)
+    spread_sums(DOWN_PARTS - 2)
     spread_sums(DOWN_PARTS - 1)
     for part in range(DOWN_PARTS):
-        arrived(recv_sem.at[4 + part], r5.at[part, other_chips])
+        arrived(spread_sem.at[part], r5.at[part, others])
         total = own_mixed[:, part * step : (part + 1) * step]
-        for peer in range(n // 2):
-            total = total + r5[part, peer].astype(jnp.float32)
+        for p in range(chips):
+            total = total + r5[part, p].astype(jnp.float32)
         out_ref[:, part * step : (part + 1) * step] = total.astype(jnp.bfloat16)
     results[0].start()
-    for stage, blocks in enumerate((s1, None, r3, r4)):
-        if blocks is not None:
-            arrived(send_sem.at[stage], blocks.at[others])
-    arrived(send_sem.at[1], t2.at[other_chips])
-    pair.wait_send()
-    for part in range(DOWN_PARTS):
-        pairs[part].wait_send()
-        arrived(send_sem.at[4 + part], t5.at[part, other_chips])
+    arrived(send_sem.at[0], s1.at[others])
+    arrived(send_sem.at[1], s2.at[others])
+    arrived(send_sem.at[2], r3.at[others])
+    arrived(send_sem.at[3], r4.at[others, 0])
+    arrived(send_sem.at[4], wqkv.at[my_rows])
+    arrived(send_sem.at[5], wo.at[core])
+    arrived(send_sem.at[6], gates_all.at[core])
+    arrived(send_sem.at[7], r4.at[:, 0])
+    arrived(send_sem.at[8], s5)
+    arrived(send_sem.at[9], t5.at[:, others])
     for c in results:
         c.wait()
 
@@ -608,13 +604,14 @@
     w_down,
 ):
     rows, width = tokens.shape
-    all_rows = rows * n
-    share = width // n
+    chips = n // 2
+    all_rows, half_rows = rows * n, rows * chips
+    share, chip_share = width // n, width // chips
     q_width, k_width = w_query.shape[1], w_key.shape[1]
     wide = q_width + k_width + w_value.shape[1]
-    stages = 4 + DOWN_PARTS
+    step = width // DOWN_PARTS
+    ff_share = w_gate.shape[1]
     anywhere = pl.BlockSpec(memory_space=pl.ANY)
-    smem = pl.BlockSpec(memory_space=pltpu.SMEM)
     bf16, f32 = jnp.bfloat16, jnp.float32
 
     def like(array):
@@ -625,10 +622,11 @@
     results = pl.pallas_call(
         functools.partial(fused, n),
         out_shape=tuple(pltpu.VMEM(shape, bf16) for shape in shapes),
-        in_specs=[anywhere, smem] + [anywhere] * 16,
+        in_specs=[anywhere] * 18,
         out_specs=(anywhere,) * 3,
         scratch_shapes=[
             like(tokens),
+            pltpu.VMEM((1, rows), lengths.dtype),
             pltpu.VMEM(routes.shape[::-1], routes.dtype),
             pltpu.VMEM(route_logits.shape[::-1], f32),
             pltpu.VMEM((1, width), f32),
@@ -637,43 +635,44 @@
             pltpu.VMEM((1, HEADS), f32),
             pltpu.VMEM((1, width), f32),
             *(pltpu.VMEM(shape, bf16) for shape in shapes),
-            like(w_query),
-            like(w_key),
-            like(w_value),
-            like(w_out),
+            pltpu.VMEM((chip_share, wide), bf16),
+            pltpu.VMEM((2, *w_out.shape), bf16),
             like(cache_key),
             like(cache_value),
             like(w_gate),
             like(w_up),
             like(w_down),
-            pltpu.VMEM((n, 2 * rows, share), bf16),
-            pltpu.VMEM((n, 2 * rows, share), bf16),
-            pltpu.VMEM((2, n // 2, rows, wide), bf16),
-            pltpu.VMEM((n // 2, rows, wide), bf16),
-            pltpu.VMEM((n // 2, rows, wide), bf16),
-            pltpu.VMEM((n // 2, rows, wide), bf16),
-            pltpu.VMEM((n, rows, q_width), bf16),
-            pltpu.VMEM((n, all_rows, share), bf16),
-            pltpu.VMEM((DOWN_PARTS, 2, n // 2, rows, width // DOWN_PARTS), bf16),
-            pltpu.VMEM((DOWN_PARTS, n // 2, rows, width // DOWN_PARTS), bf16),
-            pltpu.VMEM((DOWN_PARTS, n // 2, rows, width // DOWN_PARTS), bf16),
-            pltpu.VMEM((DOWN_PARTS, n // 2, rows, width // DOWN_PARTS), bf16),
-            pltpu.VMEM((all_rows, share), f32),
-            pltpu.VMEM((all_rows, share), f32),
-            pltpu.VMEM((all_rows, q_width), f32),
-            pltpu.VMEM((all_rows, width), bf16),
-            pltpu.VMEM((all_rows, w_gate.shape[1]), bf16),
-            pltpu.SemaphoreType.DMA((8,)),
+            pltpu.VMEM((chips, 2 * rows, chip_share), bf16),
+            pltpu.VMEM((chips, 2 * rows, chip_share), bf16),
+            pltpu.VMEM((chips, rows, wide), bf16),
+            pltpu.VMEM((chips, rows, wide), bf16),
+            pltpu.VMEM((chips, rows, q_width), bf16),
+            pltpu.VMEM((chips, 2, half_rows, chip_share), bf16),
+            pltpu.VMEM((DOWN_PARTS, half_rows, step), bf16),
+            pltpu.VMEM((DOWN_PARTS, half_rows, step), bf16),
+            pltpu.VMEM((DOWN_PARTS, half_rows, step), f32),
+            pltpu.VMEM((DOWN_PARTS, chips, rows, step), bf16),
+            pltpu.VMEM((DOWN_PARTS, chips, rows, step), bf16),
+            pltpu.VMEM((2, half_rows, 128), f32),
+            pltpu.VMEM((half_rows, chip_share), f32),
+            pltpu.VMEM((half_rows, 128), f32),
+            pltpu.VMEM((half_rows, q_width), f32),
+            pltpu.VMEM((rows, width), f32),
+            pltpu.VMEM((all_rows, ff_share), f32),
+            pltpu.VMEM((all_rows, ff_share), f32),
+            pltpu.VMEM((all_rows, ff_share), bf16),
+            pltpu.SemaphoreType.DMA((9,)),
             pltpu.SemaphoreType.DMA((3,)),
             pltpu.SemaphoreType.DMA((4,)),
-            pltpu.SemaphoreType.DMA((rows,)),
-            pltpu.SemaphoreType.DMA((rows,)),
-            pltpu.SemaphoreType.DMA((3, WEIGHT_PARTS)),
-            pltpu.SemaphoreType.DMA((stages,)),
-            pltpu.SemaphoreType.DMA((stages,)),
-            pltpu.SemaphoreType.DMA((n,)),
-            pltpu.SemaphoreType.DMA((DOWN_PARTS + 1,)),
-            pltpu.SemaphoreType.DMA((DOWN_PARTS + 1,)),
+            pltpu.SemaphoreType.DMA((2,)),
+            pltpu.SemaphoreType.DMA((3,)),
+            pltpu.SemaphoreType.DMA((10,)),
+            pltpu.SemaphoreType.DMA((3,)),
+            pltpu.SemaphoreType.DMA((chips,)),
+            pltpu.SemaphoreType.DMA((chips,)),
+            pltpu.SemaphoreType.DMA((DOWN_PARTS,)),
+            pltpu.SemaphoreType.DMA((DOWN_PARTS,)),
+            pltpu.SemaphoreType.DMA((3,)),
         ],
         compiler_params=pltpu.CompilerParams(
             collective_id=0, has_side_effects=True, vmem_limit_bytes=60 * 1024 * 1024
@@ -681,7 +680,7 @@
         cost_estimate=pl.CostEstimate(flops=flops, bytes_accessed=flops // all_rows, transcendentals=0),
     )(
         tokens,
-        lengths,
+        lengths.reshape(1, -1),
         cache_key,
         cache_value,
         routes.T,
@@ -714,7 +713,9 @@
     def body(*arrays):
         tokens, w_gate = arrays[0], arrays[15]
         share = tokens.shape[1] // n
-        if share == 128 and n & (n - 1) == 0 and w_gate.shape[1] % COLUMNS == 0:
+        aligned = share == 128 and n & (n - 1) == 0 and n % 4 == 0
+        halves = (FF // w_gate.shape[1]) % 2 == 0 and arrays[13].shape[1] == share
+        if aligned and halves and w_gate.shape[1] % COLUMNS == 0 and tokens.shape[0] * n % 64 == 0:
             return local(n, *arrays)
         return plain(*arrays)
 

time: 41.7 us -> 38.1 us (0.914)
  Pallas kernels: 40.8 us -> 37.2 us
    pallas_call x1, Pallas kernels: 40.2 us -> 36.5 us  [local(): pl.pallas_call(functools.partial(fused, n), out_shape=tuple((pltpu.VMEM(s...]
where the time goes in v1:
time: 38.1 us; the launch traced here: 37.8 us
  Pallas kernels  37.2 us (98%)
  between operations  0.65 us (2%)
    pallas_call x1, Pallas kernels, local(): pl.pallas_call(functools.partial(fused, n), out_shape=tuple((pltpu.VMEM(s...  36.5 us

profile of v1, /device:TPU:0, one launch (start us, length us, event | category | flops | bytes accessed | tf_op | source)
XLA Modules:
  0.0 37.8 jit_solution(12182171906128989945)
XLA Ops:
  0.6 36.5 %shard_map.193 = (bf16[4,2048]{1,0:T(4,128)(2,1)S(1)}, bf16[4,256]{1,0:T(4,128)(2,1)S(1)}, bf16[4,256]{1,0:T(4,128)(2,1)S(1)}) custom-call(bf16[4,2048]{1,0:T(4,128)(2,1)} %tokens_hbm.1, s32[1,4]{1,0:T(1,128)} %bitcast.12, bf16[4,1024,256]{2,1,0:T(8,128)(2,1)} %ck_hbm.1, bf16[4,1024,256]{2,1,0:T(8,128)(2,1)} %cv_hbm.1, s32[2,4]{1,0:T(2,128)} %bitcast.10, ...), custom_call_target="tpu_custom_call" | custom-call | flops 1409286144 | bytes 22020096 | tf_op jit(solution)/shard_map/pallas_call | solution.py:622
  37.2 0.6 %shard_map.194 = (bf16[4,2048]{1,0:T(4,128)(2,1)}, bf16[4,256]{1,0:T(4,128)(2,1)}, bf16[4,256]{1,0:T(4,128)(2,1)}) custom-call(bf16[4,2048]{1,0:T(4,128)(2,1)S(1)} %get-tuple-element.6.refs_0_, bf16[4,256]{1,0:T(4,128)(2,1)S(1)} %get-tuple-element.7.refs_1_, bf16[4,256]{1,0:T(4,128)(2,1)S(1)} %get-tuple-element.8.refs_2_), custom_call_target="tpu_custom_call" | custom-call | tf_op jit(solution)/shard_map/pallas_call | solution.py:701

commit v2 on v1

--- a/solution.py
+++ b/solution.py
@@ -119,6 +119,7 @@
 
 WEIGHT_PARTS = 2
 DOWN_PARTS = 4
+SCHEDULE = (0, (0,), 1, 2, 3, 4, (1,), 5, (2,), 6, (3,), 7, (4,), (5, 6), (7,))
 COLUMNS = 256
 
 
@@ -185,9 +186,11 @@
     out_ref,
     new_key_ref,
     new_value_ref,
+    wq_raw,
     wqkv,
     wo,
     ck,
+    kt,
     cv,
     wg,
     wu,
@@ -196,6 +199,9 @@
     r1,
     s2,
     r2,
+    s2kv,
+    r2kv,
+    s3,
     r3,
     r4,
     s5,
@@ -227,7 +233,8 @@
     me = lax.axis_index("ep")
     core, chip = me % 2, me // 2
     chips = n // 2
-    sibling = me + 1 - 2 * core
+    other = 1 - core
+    sibling = 2 * chip + other
     rows, width = tokens_ref.shape
     half_rows = rows * chips
     all_rows = rows * n
@@ -245,13 +252,13 @@
         bit = k.bit_length() - 1
         flip = 2**bit * (1 - 2 * ((chip // 2**bit) % 2))
         chip_at.append(chip_at[k - 2**bit] + flip)
-    peer_at = [2 * c + core for c in chip_at]
-    furthest_first = range(chips - 1, 0, -1)
-    for device in [peer_at[k] for k in furthest_first] + [sibling]:
+    peer_at = [2 * c + other for c in chip_at]
+    furthest_first = range(chips - 1, -1, -1)
+    for k in furthest_first:
         pl.semaphore_signal(
             barrier,
             inc=1,
-            device_id={"ep": device},
+            device_id={"ep": peer_at[k]},
             device_id_type=pl.DeviceIdType.MESH,
         )
 
@@ -279,13 +286,21 @@
         pltpu.make_async_copy(a, b, small_sem.at[i])
         for i, (a, b) in enumerate(
             (
-                (wq_hbm, wqkv.at[my_rows, 0:q_width]),
+                (wq_hbm, wq_raw),
                 (wk_hbm, wqkv.at[my_rows, q_width : q_width + k_width]),
                 (wv_hbm, wqkv.at[my_rows, q_width + k_width :]),
-                (wo_hbm, wo.at[core]),
             )
         )
     ]
+    for head in range(HEADS):
+        place = head % group_size * KV_HEADS + head // group_size
+        small.append(
+            pltpu.make_async_copy(
+                wo_hbm.at[head * HEAD_DIM : (head + 1) * HEAD_DIM],
+                wo.at[core, place * HEAD_DIM : (place + 1) * HEAD_DIM],
+                small_sem.at[3],
+            )
+        )
     for c in small:
         c.start()
     caches = [pltpu.make_async_copy(ck_hbm.at[b], ck.at[b], cache_sem.at[0]) for b in range(rows)]
@@ -343,18 +358,26 @@
         s1[p] = jnp.concatenate(
             [as_float[:, p * chip_share : (p + 1) * chip_share], aux], axis=0
         ).astype(jnp.bfloat16)
+    for c in small[:3]:
+        c.wait()
+    left_half = iota((share, 2 * HEAD_DIM), 1) < HEAD_DIM
+    for place in range(0, HEADS, 2):
+        halves = []
+        for side in range(2):
+            head = (place + side) % KV_HEADS * group_size + (place + side) // KV_HEADS
+            start = head // 2 * 2 * HEAD_DIM
+            half = wq_raw[:, start : start + 2 * HEAD_DIM].astype(jnp.float32)
+            halves.append(half if head % 2 == side else pltpu.roll(half, HEAD_DIM, 1))
+        wqkv[my_rows, place * HEAD_DIM : (place + 2) * HEAD_DIM] = jnp.where(
+            left_half, halves[0], halves[1]
+        ).astype(jnp.bfloat16)
     pl.semaphore_wait(barrier, chips)
     for k in furthest_first:
         send(0, peer_at[k], s1.at[chip_at[k]], r1.at[chip], recv_sem.at[0])
-    for c in small[:3]:
-        c.wait()
     send(4, sibling, wqkv.at[my_rows], wqkv.at[my_rows], twin_sem.at[0])
-    small[3].wait()
-    send(5, sibling, wo.at[core], wo.at[core], twin_sem.at[1])
     for c in caches:
         c.start()
-    r1[chip] = s1[chip]
-    arrived(recv_sem.at[0], r1.at[others])
+    arrived(recv_sem.at[0], r1)
     for c in weights:
         c.start()
     for p in range(chips):
@@ -370,110 +393,111 @@
     normed = (token_cols[...] * row_scale * my_gain).astype(jnp.bfloat16)
     arrived(twin_sem.at[0], wqkv.at[my_rows])
 
-    partial = dot(normed, wqkv[...])
+    partial = dot(normed, wqkv[:, :q_width])
     for p in range(chips):
         s2[p] = partial[p * rows : (p + 1) * rows].astype(jnp.bfloat16)
     for k in furthest_first:
         send(1, peer_at[k], s2.at[chip_at[k]], r2.at[chip], recv_sem.at[1])
-    r2[chip] = s2[chip]
+    partial = dot(normed, wqkv[:, q_width:])
+    for p in range(chips):
+        s2kv[p] = partial[p * rows : (p + 1) * rows].astype(jnp.bfloat16)
+    for k in furthest_first:
+        send(10, peer_at[k], s2kv.at[chip_at[k]], r2kv.at[chip], recv_sem.at[3])
+    arrived(small_sem.at[3], wo.at[core])
+    send(5, sibling, wo.at[core], wo.at[core], twin_sem.at[1])
     my_gate = jnp.sum(
         jnp.where((lane < 3 * EXPERTS) & (lane % EXPERTS == my_expert), aux, 0.0),
         axis=1,
         keepdims=True,
     )
-    gates_all[core] = jnp.broadcast_to(my_gate, aux.shape)
-    send(6, sibling, gates_all.at[core], gates_all.at[core], twin_sem.at[2])
-
-    head_of_lane = iota((HEADS, q_width), 1) // HEAD_DIM
-    own_lane = head_of_lane == iota((HEADS, q_width), 0)
-    source_lane = iota((q_width, k_width), 0)
-    target_lane = iota((q_width, k_width), 1)
-    fold = jnp.where(
-        (source_lane // (HEAD_DIM * group_size) == target_lane // HEAD_DIM)
-        & (source_lane % HEAD_DIM == target_lane % HEAD_DIM),
+    gates_all[other] = jnp.broadcast_to(my_gate, aux.shape)
+    send(6, sibling, gates_all.at[other], gates_all.at[other], twin_sem.at[2])
+
+    own_group = iota((HEADS, k_width), 1) // HEAD_DIM == iota((HEADS, k_width), 0) % KV_HEADS
+    later = jnp.where(
+        iota((COLUMNS, COLUMNS), 0) > iota((COLUMNS, COLUMNS), 1), 1.0, 0.0
+    ).astype(jnp.bfloat16)
+    query_gain = jnp.concatenate([query_gain_ref[...]] * KV_HEADS, axis=1)
+    key_gain = jnp.concatenate([key_gain_ref[...]] * KV_HEADS, axis=1)
+    blocks = cache_len // COLUMNS
+    head_rows = rows * HEADS
+    place, head = iota((HEADS, HEADS), 0), iota((HEADS, HEADS), 1)
+    head_bias = jnp.where(
+        head == place % KV_HEADS * group_size + place // KV_HEADS,
+        jnp.broadcast_to(head_bias_ref[...], head.shape),
+        0.0,
+    )
+    head_bias = jnp.concatenate([jnp.sum(head_bias, axis=1, keepdims=True)] * rows, axis=0)
+    out_row, in_row = iota((group_size * rows, head_rows), 0), iota((group_size * rows, head_rows), 1)
+    gather = jnp.where(
+        (out_row % rows == in_row // HEADS) & (out_row // rows == in_row % HEADS // KV_HEADS),
         1.0,
         0.0,
     ).astype(jnp.bfloat16)
-    later = jnp.where(
-        iota((COLUMNS, COLUMNS), 0) > iota((COLUMNS, COLUMNS), 1), 1.0, 0.0
-    ).astype(jnp.bfloat16)
-    query_gain = jnp.concatenate([query_gain_ref[...]] * HEADS, axis=1)
-    key_gain = jnp.concatenate([key_gain_ref[...]] * KV_HEADS, axis=1)
-    blocks = cache_len // COLUMNS
-    head_rows = rows * HEADS
-    head_bias = jnp.concatenate([column(head_bias_ref[...])] * rows, axis=0)
     row_of = iota((head_rows, 1), 0) // HEADS
     lengths = jnp.zeros((head_rows, 1), jnp.int32)
     for b in range(rows):
         lengths = jnp.where(row_of == b, lengths_ref[:, b : b + 1], lengths)
     live = iota((head_rows, cache_len), 1) < lengths
     arrived(cache_sem.at[0], ck)
+    for b in range(rows):
+        kt[b] = ck[b].T
     arrived(cache_sem.at[1], cv)
 
-    arrived(recv_sem.at[1], r2.at[others])
+    arrived(recv_sem.at[1], r2)
     total = r2[0].astype(jnp.float32)
     for p in range(1, chips):
         total = total + r2[p].astype(jnp.float32)
-    queries = total[:, :q_width]
+    queries = total
     spread = []
     for b in range(rows):
-        wide = jnp.where(own_lane, jnp.broadcast_to(queries[b : b + 1], own_lane.shape), 0.0)
+        wide = [
+            jnp.broadcast_to(
+                queries[b : b + 1, i * k_width : (i + 1) * k_width], (KV_HEADS, k_width)
+            )
+            for i in range(group_size)
+        ]
+        wide = jnp.where(own_group, jnp.concatenate(wide, axis=0), 0.0)
         mean = jnp.sum(wide * wide, axis=1, keepdims=True) / HEAD_DIM
         spread.append((wide * lax.rsqrt(mean + EPSILON) * query_gain).astype(jnp.bfloat16))
-    folded = dot(jnp.concatenate(spread, axis=0), fold).astype(jnp.bfloat16)
-    scores = jnp.concatenate(
-        [
-            lax.dot_general(
-                folded[b * HEADS : (b + 1) * HEADS],
-                ck[b],
-                (((1,), (1,)), ((), ())),
-                preferred_element_type=jnp.float32,
-            )
-            for b in range(rows)
-        ],
-        axis=0,
-    )
+    scores = jnp.concatenate([dot(spread[b], kt[b]) for b in range(rows)], axis=0)
     scores = scores * HEAD_DIM ** (-0.5) + head_bias
-    tail_log = jnp.log1p(jnp.exp(-jnp.abs(scores)))
+    tail_log = jnp.log(1.0 + jnp.exp(-jnp.abs(scores)))
     remain = jnp.where(live, jnp.minimum(-scores, 0.0) - tail_log, 0.0)
+    pieces = [remain[:, i * COLUMNS : (i + 1) * COLUMNS] for i in range(blocks)]
+    highs = [block.astype(jnp.bfloat16) for block in pieces]
+    lows = [
+        (block - high.astype(jnp.float32)).astype(jnp.bfloat16)
+        for block, high in zip(pieces, highs)
+    ]
+    sums = dot(jnp.concatenate(highs + lows, axis=0), later)
     after = [None] * blocks
     carry = jnp.zeros((head_rows, 1), jnp.float32)
     for i in reversed(range(blocks)):
-        block = remain[:, i * COLUMNS : (i + 1) * COLUMNS]
-        high = block.astype(jnp.bfloat16)
-        low = (block - high.astype(jnp.float32)).astype(jnp.bfloat16)
-        after[i] = dot(high, later) + dot(low, later) + carry
-        carry = carry + jnp.sum(block, axis=1, keepdims=True)
+        low = (blocks + i) * head_rows
+        after[i] = (
+            sums[i * head_rows : (i + 1) * head_rows] + sums[low : low + head_rows] + carry
+        )
+        carry = carry + jnp.sum(pieces[i], axis=1, keepdims=True)
     after_sum = jnp.concatenate(after, axis=1)
     chance = jnp.exp(jnp.minimum(scores, 0.0) - tail_log + after_sum)
     weight = jnp.where(live, chance, 0.0).astype(jnp.bfloat16)
     mixed_heads = jnp.concatenate(
         [dot(weight[b * HEADS : (b + 1) * HEADS], cv[b]) for b in range(rows)], axis=0
     )
-    own_group = (
-        iota((head_rows, k_width), 1) // HEAD_DIM
-        == iota((head_rows, k_width), 0) % HEADS // group_size
-    )
-    heads = jnp.where(own_group, mixed_heads, 0.0).astype(jnp.bfloat16)
-    unfolded = lax.dot_general(
-        heads,
-        fold,
-        (((1,), (1,)), ((), ())),
-        preferred_element_type=jnp.float32,
-    )
-    attended = [
-        jnp.sum(
-            jnp.where(own_lane, unfolded[b * HEADS : (b + 1) * HEADS], 0.0), axis=0, keepdims=True
-        )
-        for b in range(rows)
-    ]
-    r3[chip] = jnp.concatenate(attended, axis=0).astype(jnp.bfloat16)
+    own_groups = jnp.concatenate([own_group] * rows, axis=0)
+    heads = jnp.where(own_groups, mixed_heads, 0.0).astype(jnp.bfloat16)
+    s3[...] = dot(gather, heads).astype(jnp.bfloat16)
 
     for k in furthest_first:
-        send(2, peer_at[k], r3.at[chip], r3.at[chip], recv_sem.at[2])
-
-    fresh_key = total[:, q_width : q_width + k_width]
-    new_value_ref[...] = total[:, q_width + k_width :].astype(jnp.bfloat16)
+        send(2, peer_at[k], s3, r3.at[chip], recv_sem.at[2])
+
+    arrived(recv_sem.at[3], r2kv)
+    total = r2kv[0].astype(jnp.float32)
+    for p in range(1, chips):
+        total = total + r2kv[p].astype(jnp.float32)
+    fresh_key = total[:, :k_width]
+    new_value_ref[...] = total[:, k_width:].astype(jnp.bfloat16)
     squares = fresh_key * fresh_key
     key_lane = iota(squares.shape, 1) // HEAD_DIM
     key_scale = jnp.zeros_like(squares)
@@ -486,45 +510,52 @@
     arrived(twin_sem.at[1], wo.at[core])
     arrived(twin_sem.at[2], gates_all.at[core])
 
-    arrived(recv_sem.at[2], r3.at[others])
+    arrived(recv_sem.at[2], r3)
     for p in range(chips):
-        attended_rows[p * rows : (p + 1) * rows, :] = r3[p].astype(jnp.float32)
+        block = r3[p].astype(jnp.float32)
+        for i in range(group_size):
+            attended_rows[p * rows : (p + 1) * rows, i * k_width : (i + 1) * k_width] = block[
+                i * rows : (i + 1) * rows
+            ]
     attended_all = attended_rows[...].astype(jnp.bfloat16)
     for h in range(2):
         columns = slice(h * share, (h + 1) * share)
         mixed = token_cols[:, columns] + dot(attended_all, wo[h])
-        r4[chip, core, :, columns] = mixed.astype(jnp.bfloat16)
-
-    mine = r4.at[chip, core]
-    for k in furthest_first:
+        r4[chip, other, :, columns] = mixed.astype(jnp.bfloat16)
+
+    mine = r4.at[chip, other]
+    for k in range(chips):
         send(3, peer_at[k], mine, mine, direct_sem.at[k])
-    send(7, sibling, mine, mine, relay_sem.at[0])
     pick = jnp.where(
         iota((8, half_rows), 1) == iota((8, half_rows), 0) + chip * rows, 1.0, 0.0
     ).astype(jnp.bfloat16)
     squares = jnp.zeros((all_rows, chip_share), jnp.float32)
     gate_column = gates_all[...].reshape(all_rows, 128)[:, :1]
-    for which, b in enumerate((wg, wu, wd)):
+    for which, b in enumerate((wg, wu)):
         arrived(weight_sem.at[which], b)
-
-    def chunk(k, squares):
-        source = chip_at[k]
-        columns = pl.ds(pl.multiple_of(source * chip_share, chip_share), chip_share)
-        arrived(relay_sem.at[k], r4.at[source, core])
-        own_mixed[:, columns] = dot(pick, r4[source, core])[:rows]
-        block = r4[source].reshape(all_rows, chip_share).astype(jnp.float32)
-        squares = squares + block * block
-        entry = (block * ffn_gain_ref[:, columns]).astype(jnp.bfloat16)
-        if k == chips - 1:
+    arrived(weight_sem.at[2], wd)
+
+    def chunks_of(group, squares, first, last):
+        entries = []
+        for k in group:
+            source = chip_at[k]
+            columns = pl.ds(pl.multiple_of(source * chip_share, chip_share), chip_share)
+            if k:
+                arrived(relay_sem.at[k - 1], r4.at[source, other])
+            own_mixed[:, columns] = dot(pick, r4[source, core])[:rows]
+            block = r4[source].reshape(all_rows, chip_share).astype(jnp.float32)
+            squares = squares + block * block
+            entries.append((columns, (block * ffn_gain_ref[:, columns]).astype(jnp.bfloat16)))
+        if last:
             scale = lax.rsqrt(jnp.sum(squares, axis=1, keepdims=True) / width + EPSILON)
         for i in range(ff_share // COLUMNS):
             inner = slice(i * COLUMNS, (i + 1) * COLUMNS)
-            gate_value = dot(entry, wg[columns, inner])
-            up_value = dot(entry, wu[columns, inner])
-            if k:
+            gate_value = sum(dot(entry, wg[columns, inner]) for columns, entry in entries)
+            up_value = sum(dot(entry, wu[columns, inner]) for columns, entry in entries)
+            if not first:
                 gate_value = gate_value + gate_acc[:, inner]
                 up_value = up_value + up_acc[:, inner]
-            if k == chips - 1:
+            if last:
                 gate_value = gate_value * scale
                 silu = gate_value / (1.0 + jnp.exp(-gate_value))
                 hidden[:, inner] = (silu * (up_value * scale) * gate_column).astype(jnp.bfloat16)
@@ -533,12 +564,14 @@
                 up_acc[:, inner] = up_value
         return squares
 
-    for k in range(1, chips):
-        block = r4.at[chip_at[k], core]
-        arrived(direct_sem.at[k], block)
-        send(7, sibling, block, block, relay_sem.at[k])
-        squares = chunk(k - 1, squares)
-    squares = chunk(chips - 1, squares)
+    for i, step in enumerate(SCHEDULE):
+        if isinstance(step, int):
+            block = r4.at[chip_at[step], core]
+            arrived(direct_sem.at[step], block)
+            if step:
+                send(7, sibling, block, block, relay_sem.at[step - 1])
+        else:
+            squares = chunks_of(step, squares, step[0] == 0, i == len(SCHEDULE) - 1)
 
     step = width // DOWN_PARTS
 
@@ -547,37 +580,37 @@
         both = own5[part] + p5[part].astype(jnp.float32)
         for p in range(chips):
             t5[part, p] = both[p * rows : (p + 1) * rows].astype(jnp.bfloat16)
-        for k in furthest_first:
+        for k in range(chips):
             send(9, peer_at[k], t5.at[part, chip_at[k]], r5.at[part, chip], spread_sem.at[part])
-        r5[part, chip] = t5[part, chip]
 
     for part in range(DOWN_PARTS):
         partial = dot(hidden[...], wd[:, part * step : (part + 1) * step])
         lower, upper = partial[:half_rows], partial[half_rows:]
-        own5[part] = jnp.where(core == 0, lower, upper)
-        s5[part] = jnp.where(core == 0, upper, lower).astype(jnp.bfloat16)
+        own5[part] = jnp.where(core == 0, upper, lower)
+        s5[part] = jnp.where(core == 0, lower, upper).astype(jnp.bfloat16)
         send(8, sibling, s5.at[part], p5.at[part], pair_sem.at[part])
         if part > 1:
             spread_sums(part - 2)
     spread_sums(DOWN_PARTS - 2)
     spread_sums(DOWN_PARTS - 1)
     for part in range(DOWN_PARTS):
-        arrived(spread_sem.at[part], r5.at[part, others])
+        arrived(spread_sem.at[part], r5.at[part])
         total = own_mixed[:, part * step : (part + 1) * step]
         for p in range(chips):
             total = total + r5[part, p].astype(jnp.float32)
         out_ref[:, part * step : (part + 1) * step] = total.astype(jnp.bfloat16)
     results[0].start()
-    arrived(send_sem.at[0], s1.at[others])
-    arrived(send_sem.at[1], s2.at[others])
-    arrived(send_sem.at[2], r3.at[others])
-    arrived(send_sem.at[3], r4.at[others, 0])
+    arrived(send_sem.at[0], s1)
+    arrived(send_sem.at[1], s2)
+    arrived(send_sem.at[10], s2kv)
+    arrived(send_sem.at[2], r3)
+    arrived(send_sem.at[3], r4.at[:, 0])
     arrived(send_sem.at[4], wqkv.at[my_rows])
     arrived(send_sem.at[5], wo.at[core])
-    arrived(send_sem.at[6], gates_all.at[core])
-    arrived(send_sem.at[7], r4.at[:, 0])
+    arrived(send_sem.at[6], gates_all.at[other])
+    arrived(send_sem.at[7], r4.at[others, 0])
     arrived(send_sem.at[8], s5)
-    arrived(send_sem.at[9], t5.at[:, others])
+    arrived(send_sem.at[9], t5)
     for c in results:
         c.wait()
 
@@ -635,18 +668,23 @@
             pltpu.VMEM((1, HEADS), f32),
             pltpu.VMEM((1, width), f32),
             *(pltpu.VMEM(shape, bf16) for shape in shapes),
+            like(w_query),
             pltpu.VMEM((chip_share, wide), bf16),
             pltpu.VMEM((2, *w_out.shape), bf16),
             like(cache_key),
+            pltpu.VMEM((rows, k_width, cache_key.shape[1]), bf16),
             like(cache_value),
             like(w_gate),
             like(w_up),
             like(w_down),
             pltpu.VMEM((chips, 2 * rows, chip_share), bf16),
             pltpu.VMEM((chips, 2 * rows, chip_share), bf16),
-            pltpu.VMEM((chips, rows, wide), bf16),
-            pltpu.VMEM((chips, rows, wide), bf16),
             pltpu.VMEM((chips, rows, q_width), bf16),
+            pltpu.VMEM((chips, rows, q_width), bf16),
+            pltpu.VMEM((chips, rows, wide - q_width), bf16),
+            pltpu.VMEM((chips, rows, wide - q_width), bf16),
+            pltpu.VMEM((rows * q_width // k_width, k_width), bf16),
+            pltpu.VMEM((chips, rows * q_width // k_width, k_width), bf16),
             pltpu.VMEM((chips, 2, half_rows, chip_share), bf16),
             pltpu.VMEM((DOWN_PARTS, half_rows, step), bf16),
             pltpu.VMEM((DOWN_PARTS, half_rows, step), bf16),
@@ -666,10 +704,10 @@
             pltpu.SemaphoreType.DMA((4,)),
             pltpu.SemaphoreType.DMA((2,)),
             pltpu.SemaphoreType.DMA((3,)),
-            pltpu.SemaphoreType.DMA((10,)),
-            pltpu.SemaphoreType.DMA((3,)),
+            pltpu.SemaphoreType.DMA((11,)),
+            pltpu.SemaphoreType.DMA((4,)),
             pltpu.SemaphoreType.DMA((chips,)),
-            pltpu.SemaphoreType.DMA((chips,)),
+            pltpu.SemaphoreType.DMA((chips - 1,)),
             pltpu.SemaphoreType.DMA((DOWN_PARTS,)),
             pltpu.SemaphoreType.DMA((DOWN_PARTS,)),
             pltpu.SemaphoreType.DMA((3,)),

time: 38.1 us -> 33.6 us (0.88)
  Pallas kernels: 37.2 us -> 32.8 us
    pallas_call x1, Pallas kernels: 36.5 us -> 32.1 us  [local(): pl.pallas_call(functools.partial(fused, n), out_shape=tuple((pltpu.VMEM(s...]
where the time goes in v2:
time: 33.6 us; the launch traced here: 33.4 us
  Pallas kernels  32.8 us (98%)
  between operations  0.65 us (2%)
    pallas_call x1, Pallas kernels, local(): pl.pallas_call(functools.partial(fused, n), out_shape=tuple((pltpu.VMEM(s...  32.1 us

profile of v2, /device:TPU:0, one launch (start us, length us, event | category | flops | bytes accessed | tf_op | source)
XLA Modules:
  0.0 33.4 jit_solution(11309682787288722610)
XLA Ops:
  0.6 32.1 %shard_map.193 = (bf16[4,2048]{1,0:T(4,128)(2,1)S(1)}, bf16[4,256]{1,0:T(4,128)(2,1)S(1)}, bf16[4,256]{1,0:T(4,128)(2,1)S(1)}) custom-call(bf16[4,2048]{1,0:T(4,128)(2,1)} %tokens_hbm.1, s32[1,4]{1,0:T(1,128)} %bitcast.12, bf16[4,1024,256]{2,1,0:T(8,128)(2,1)} %ck_hbm.1, bf16[4,1024,256]{2,1,0:T(8,128)(2,1)} %cv_hbm.1, s32[2,4]{1,0:T(2,128)} %bitcast.10, ...), custom_call_target="tpu_custom_call" | custom-call | flops 1409286144 | bytes 22020096 | tf_op jit(solution)/shard_map/pallas_call | solution.py:655
  32.8 0.6 %shard_map.194 = (bf16[4,2048]{1,0:T(4,128)(2,1)}, bf16[4,256]{1,0:T(4,128)(2,1)}, bf16[4,256]{1,0:T(4,128)(2,1)}) custom-call(bf16[4,2048]{1,0:T(4,128)(2,1)S(1)} %get-tuple-element.6.refs_0_, bf16[4,256]{1,0:T(4,128)(2,1)S(1)} %get-tuple-element.7.refs_1_, bf16[4,256]{1,0:T(4,128)(2,1)S(1)} %get-tuple-element.8.refs_2_), custom_call_target="tpu_custom_call" | custom-call | tf_op jit(solution)/shard_map/pallas_call | solution.py:739

commit v3 on v2

--- a/solution.py
+++ b/solution.py
@@ -118,7 +118,8 @@
 
 
 WEIGHT_PARTS = 2
-DOWN_PARTS = 4
+PAIR_LAG = 2
+DOWN_WIDTHS = (512, 512, 512, 512)
 SCHEDULE = (0, (0,), 1, 2, 3, 4, (1,), 5, (2,), 6, (3,), 7, (4,), (5, 6), (7,))
 COLUMNS = 256
 
@@ -218,10 +219,7 @@
     up_acc,
     hidden,
     operand_sem,
-    result_sem,
     small_sem,
-    cache_sem,
-    weight_sem,
     send_sem,
     recv_sem,
     direct_sem,
@@ -303,17 +301,17 @@
         )
     for c in small:
         c.start()
-    caches = [pltpu.make_async_copy(ck_hbm.at[b], ck.at[b], cache_sem.at[0]) for b in range(rows)]
-    caches += [pltpu.make_async_copy(cv_hbm.at[b], cv.at[b], cache_sem.at[1]) for b in range(rows)]
+    caches = [pltpu.make_async_copy(ck_hbm.at[b], ck.at[b], operand_sem.at[0]) for b in range(rows)]
+    caches += [pltpu.make_async_copy(cv_hbm.at[b], cv.at[b], operand_sem.at[1]) for b in range(rows)]
     weights = []
     for which, (a, b) in enumerate(((wg_hbm, wg), (wu_hbm, wu), (wd_hbm, wd))):
         step = b.shape[0] // WEIGHT_PARTS
         for part in range(WEIGHT_PARTS):
             piece = pl.ds(part * step, step)
-            weights.append(pltpu.make_async_copy(a.at[piece], b.at[piece], weight_sem.at[which]))
+            weights.append(pltpu.make_async_copy(a.at[piece], b.at[piece], operand_sem.at[2 + which]))
 
     results = [
-        pltpu.make_async_copy(a, b, result_sem.at[i])
+        pltpu.make_async_copy(a, b, operand_sem.at[5 + i])
         for i, (a, b) in enumerate(
             ((out_ref, out_any), (new_key_ref, new_key_any), (new_value_ref, new_value_any))
         )
@@ -374,7 +372,8 @@
     pl.semaphore_wait(barrier, chips)
     for k in furthest_first:
         send(0, peer_at[k], s1.at[chip_at[k]], r1.at[chip], recv_sem.at[0])
-    send(4, sibling, wqkv.at[my_rows], wqkv.at[my_rows], twin_sem.at[0])
+    query_half = wqkv.at[my_rows, 0:q_width]
+    send(4, sibling, query_half, query_half, twin_sem.at[0])
     for c in caches:
         c.start()
     arrived(recv_sem.at[0], r1)
@@ -391,27 +390,22 @@
     )
     my_gain = mix_gain_ref[:, pl.ds(pl.multiple_of(chip * chip_share, chip_share), chip_share)]
     normed = (token_cols[...] * row_scale * my_gain).astype(jnp.bfloat16)
-    arrived(twin_sem.at[0], wqkv.at[my_rows])
+    arrived(twin_sem.at[0], query_half)
 
     partial = dot(normed, wqkv[:, :q_width])
     for p in range(chips):
         s2[p] = partial[p * rows : (p + 1) * rows].astype(jnp.bfloat16)
     for k in furthest_first:
         send(1, peer_at[k], s2.at[chip_at[k]], r2.at[chip], recv_sem.at[1])
-    partial = dot(normed, wqkv[:, q_width:])
-    for p in range(chips):
-        s2kv[p] = partial[p * rows : (p + 1) * rows].astype(jnp.bfloat16)
-    for k in furthest_first:
-        send(10, peer_at[k], s2kv.at[chip_at[k]], r2kv.at[chip], recv_sem.at[3])
-    arrived(small_sem.at[3], wo.at[core])
-    send(5, sibling, wo.at[core], wo.at[core], twin_sem.at[1])
+    key_value_half = wqkv.at[my_rows, q_width:]
+    send(3, sibling, key_value_half, key_value_half, twin_sem.at[3])
     my_gate = jnp.sum(
         jnp.where((lane < 3 * EXPERTS) & (lane % EXPERTS == my_expert), aux, 0.0),
         axis=1,
         keepdims=True,
     )
     gates_all[other] = jnp.broadcast_to(my_gate, aux.shape)
-    send(6, sibling, gates_all.at[other], gates_all.at[other], twin_sem.at[2])
+    send(5, sibling, gates_all.at[other], gates_all.at[other], twin_sem.at[2])
 
     own_group = iota((HEADS, k_width), 1) // HEAD_DIM == iota((HEADS, k_width), 0) % KV_HEADS
     later = jnp.where(
@@ -439,12 +433,21 @@
     for b in range(rows):
         lengths = jnp.where(row_of == b, lengths_ref[:, b : b + 1], lengths)
     live = iota((head_rows, cache_len), 1) < lengths
-    arrived(cache_sem.at[0], ck)
+    arrived(operand_sem.at[0], ck)
     for b in range(rows):
         kt[b] = ck[b].T
-    arrived(cache_sem.at[1], cv)
-
+    arrived(operand_sem.at[1], cv)
+
+    arrived(twin_sem.at[3], key_value_half)
+    partial = dot(normed, wqkv[:, q_width:])
+    for p in range(chips):
+        s2kv[p] = partial[p * rows : (p + 1) * rows].astype(jnp.bfloat16)
     arrived(recv_sem.at[1], r2)
+    for k in furthest_first:
+        send(2, peer_at[k], s2kv.at[chip_at[k]], r2kv.at[chip], recv_sem.at[3])
+    arrived(small_sem.at[3], wo.at[core])
+    arrived(send_sem.at[4], query_half)
+    send(4, sibling, wo.at[core], wo.at[core], twin_sem.at[1])
     total = r2[0].astype(jnp.float32)
     for p in range(1, chips):
         total = total + r2[p].astype(jnp.float32)
@@ -489,24 +492,10 @@
     heads = jnp.where(own_groups, mixed_heads, 0.0).astype(jnp.bfloat16)
     s3[...] = dot(gather, heads).astype(jnp.bfloat16)
 
+    arrived(send_sem.at[0], s1)
     for k in furthest_first:
-        send(2, peer_at[k], s3, r3.at[chip], recv_sem.at[2])
-
-    arrived(recv_sem.at[3], r2kv)
-    total = r2kv[0].astype(jnp.float32)
-    for p in range(1, chips):
-        total = total + r2kv[p].astype(jnp.float32)
-    fresh_key = total[:, :k_width]
-    new_value_ref[...] = total[:, k_width:].astype(jnp.bfloat16)
-    squares = fresh_key * fresh_key
-    key_lane = iota(squares.shape, 1) // HEAD_DIM
-    key_scale = jnp.zeros_like(squares)
-    for g in range(KV_HEADS):
-        mean = jnp.sum(jnp.where(key_lane == g, squares, 0.0), axis=1, keepdims=True) / HEAD_DIM
-        key_scale = jnp.where(key_lane == g, lax.rsqrt(mean + EPSILON), key_scale)
-    new_key_ref[...] = (fresh_key * key_scale * key_gain).astype(jnp.bfloat16)
-    for c in results[1:]:
-        c.start()
+        send(0, peer_at[k], s3, r3.at[chip], recv_sem.at[2])
+
     arrived(twin_sem.at[1], wo.at[core])
     arrived(twin_sem.at[2], gates_all.at[core])
 
@@ -524,16 +513,18 @@
         r4[chip, other, :, columns] = mixed.astype(jnp.bfloat16)
 
     mine = r4.at[chip, other]
+    arrived(send_sem.at[1], s2)
+    arrived(send_sem.at[5], gates_all.at[other])
     for k in range(chips):
-        send(3, peer_at[k], mine, mine, direct_sem.at[k])
+        send(1, peer_at[k], mine, mine, direct_sem.at[k])
     pick = jnp.where(
         iota((8, half_rows), 1) == iota((8, half_rows), 0) + chip * rows, 1.0, 0.0
     ).astype(jnp.bfloat16)
     squares = jnp.zeros((all_rows, chip_share), jnp.float32)
     gate_column = gates_all[...].reshape(all_rows, 128)[:, :1]
     for which, b in enumerate((wg, wu)):
-        arrived(weight_sem.at[which], b)
-    arrived(weight_sem.at[2], wd)
+        arrived(operand_sem.at[2 + which], b)
+    arrived(operand_sem.at[4], wd)
 
     def chunks_of(group, squares, first, last):
         entries = []
@@ -564,53 +555,90 @@
                 up_acc[:, inner] = up_value
         return squares
 
+    def finish_key_value():
+        arrived(recv_sem.at[3], r2kv)
+        total = r2kv[0].astype(jnp.float32)
+        for p in range(1, chips):
+            total = total + r2kv[p].astype(jnp.float32)
+        fresh_key = total[:, :k_width]
+        new_value_ref[...] = total[:, k_width:].astype(jnp.bfloat16)
+        key_squares = fresh_key * fresh_key
+        key_lane = iota(key_squares.shape, 1) // HEAD_DIM
+        key_scale = jnp.zeros_like(key_squares)
+        for g in range(KV_HEADS):
+            mean = jnp.sum(jnp.where(key_lane == g, key_squares, 0.0), axis=1, keepdims=True) / HEAD_DIM
+            key_scale = jnp.where(key_lane == g, lax.rsqrt(mean + EPSILON), key_scale)
+        new_key_ref[...] = (fresh_key * key_scale * key_gain).astype(jnp.bfloat16)
+        for c in results[1:]:
+            c.start()
+
     for i, step in enumerate(SCHEDULE):
+        if i == 2:
+            finish_key_value()
         if isinstance(step, int):
             block = r4.at[chip_at[step], core]
             arrived(direct_sem.at[step], block)
             if step:
-                send(7, sibling, block, block, relay_sem.at[step - 1])
+                send(6, sibling, block, block, relay_sem.at[step - 1])
         else:
             squares = chunks_of(step, squares, step[0] == 0, i == len(SCHEDULE) - 1)
 
-    step = width // DOWN_PARTS
+    parts = len(DOWN_WIDTHS)
+    starts = [sum(DOWN_WIDTHS[:part]) for part in range(parts)]
 
     def spread_sums(part):
-        arrived(pair_sem.at[part], p5.at[part])
-        both = own5[part] + p5[part].astype(jnp.float32)
+        lanes = pl.ds(0, DOWN_WIDTHS[part])
+        arrived(pair_sem.at[part], p5.at[part, :, lanes])
+        both = own5[part, :, lanes] + p5[part, :, lanes].astype(jnp.float32)
         for p in range(chips):
-            t5[part, p] = both[p * rows : (p + 1) * rows].astype(jnp.bfloat16)
+            t5[part, p, :, lanes] = both[p * rows : (p + 1) * rows].astype(jnp.bfloat16)
         for k in range(chips):
-            send(9, peer_at[k], t5.at[part, chip_at[k]], r5.at[part, chip], spread_sem.at[part])
-
-    for part in range(DOWN_PARTS):
-        partial = dot(hidden[...], wd[:, part * step : (part + 1) * step])
+            send(
+                7,
+                peer_at[k],
+                t5.at[part, chip_at[k], :, lanes],
+                r5.at[part, chip, :, lanes],
+                spread_sem.at[part],
+            )
+
+    def down_product(start, lanes):
+        return jnp.concatenate(
+            [
+                dot(hidden[...], wd[:, start + i : start + i + COLUMNS])
+                for i in range(0, lanes, COLUMNS)
+            ],
+            axis=1,
+        )
+
+    for part in range(parts):
+        lanes = pl.ds(0, DOWN_WIDTHS[part])
+        partial = down_product(starts[part], DOWN_WIDTHS[part])
         lower, upper = partial[:half_rows], partial[half_rows:]
-        own5[part] = jnp.where(core == 0, upper, lower)
-        s5[part] = jnp.where(core == 0, lower, upper).astype(jnp.bfloat16)
-        send(8, sibling, s5.at[part], p5.at[part], pair_sem.at[part])
-        if part > 1:
-            spread_sums(part - 2)
-    spread_sums(DOWN_PARTS - 2)
-    spread_sums(DOWN_PARTS - 1)
-    for part in range(DOWN_PARTS):
-        arrived(spread_sem.at[part], r5.at[part])
-        total = own_mixed[:, part * step : (part + 1) * step]
+        own5[part, :, lanes] = jnp.where(core == 0, upper, lower)
+        s5[part, :, lanes] = jnp.where(core == 0, lower, upper).astype(jnp.bfloat16)
+        send(5, sibling, s5.at[part, :, lanes], p5.at[part, :, lanes], pair_sem.at[part])
+        if part >= PAIR_LAG:
+            spread_sums(part - PAIR_LAG)
+    for part in range(parts - PAIR_LAG, parts):
+        spread_sums(part)
+    for part in range(parts):
+        lanes = pl.ds(0, DOWN_WIDTHS[part])
+        columns = slice(starts[part], starts[part] + DOWN_WIDTHS[part])
+        arrived(spread_sem.at[part], r5.at[part, :, :, lanes])
+        total = own_mixed[:, columns]
         for p in range(chips):
-            total = total + r5[part, p].astype(jnp.float32)
-        out_ref[:, part * step : (part + 1) * step] = total.astype(jnp.bfloat16)
+            total = total + r5[part, p, :, lanes].astype(jnp.float32)
+        out_ref[:, columns] = total.astype(jnp.bfloat16)
     results[0].start()
-    arrived(send_sem.at[0], s1)
-    arrived(send_sem.at[1], s2)
-    arrived(send_sem.at[10], s2kv)
-    arrived(send_sem.at[2], r3)
-    arrived(send_sem.at[3], r4.at[:, 0])
-    arrived(send_sem.at[4], wqkv.at[my_rows])
-    arrived(send_sem.at[5], wo.at[core])
-    arrived(send_sem.at[6], gates_all.at[other])
-    arrived(send_sem.at[7], r4.at[others, 0])
-    arrived(send_sem.at[8], s5)
-    arrived(send_sem.at[9], t5)
+    arrived(send_sem.at[2], s2kv)
+    arrived(send_sem.at[3], key_value_half)
+    arrived(send_sem.at[0], r3)
+    arrived(send_sem.at[1], r4.at[:, 0])
+    arrived(send_sem.at[4], wo.at[core])
+    arrived(send_sem.at[6], r4.at[others, 0])
+    whole = pl.ds(0, width // s5.shape[2])
+    arrived(send_sem.at[5], s5.at[whole])
+    arrived(send_sem.at[7], t5.at[whole])
     for c in results:
         c.wait()
 
@@ -642,7 +670,7 @@
     share, chip_share = width // n, width // chips
     q_width, k_width = w_query.shape[1], w_key.shape[1]
     wide = q_width + k_width + w_value.shape[1]
-    step = width // DOWN_PARTS
+    parts, step = len(DOWN_WIDTHS), max(DOWN_WIDTHS)
     ff_share = w_gate.shape[1]
     anywhere = pl.BlockSpec(memory_space=pl.ANY)
     bf16, f32 = jnp.bfloat16, jnp.float32
@@ -686,11 +714,11 @@
             pltpu.VMEM((rows * q_width // k_width, k_width), bf16),
             pltpu.VMEM((chips, rows * q_width // k_width, k_width), bf16),
             pltpu.VMEM((chips, 2, half_rows, chip_share), bf16),
-            pltpu.VMEM((DOWN_PARTS, half_rows, step), bf16),
-            pltpu.VMEM((DOWN_PARTS, half_rows, step), bf16),
-            pltpu.VMEM((DOWN_PARTS, half_rows, step), f32),
-            pltpu.VMEM((DOWN_PARTS, chips, rows, step), bf16),
-            pltpu.VMEM((DOWN_PARTS, chips, rows, step), bf16),
+            pltpu.VMEM((parts, half_rows, step), bf16),
+            pltpu.VMEM((parts, half_rows, step), bf16),
+            pltpu.VMEM((parts, half_rows, step), f32),
+            pltpu.VMEM((parts, chips, rows, step), bf16),
+            pltpu.VMEM((parts, chips, rows, step), bf16),
             pltpu.VMEM((2, half_rows, 128), f32),
             pltpu.VMEM((half_rows, chip_share), f32),
             pltpu.VMEM((half_rows, 128), f32),
@@ -700,17 +728,14 @@
             pltpu.VMEM((all_rows, ff_share), f32),
             pltpu.VMEM((all_rows, ff_share), bf16),
             pltpu.SemaphoreType.DMA((9,)),
-            pltpu.SemaphoreType.DMA((3,)),
             pltpu.SemaphoreType.DMA((4,)),
-            pltpu.SemaphoreType.DMA((2,)),
-            pltpu.SemaphoreType.DMA((3,)),
-            pltpu.SemaphoreType.DMA((11,)),
+            pltpu.SemaphoreType.DMA((8,)),
             pltpu.SemaphoreType.DMA((4,)),
             pltpu.SemaphoreType.DMA((chips,)),
             pltpu.SemaphoreType.DMA((chips - 1,)),
-            pltpu.SemaphoreType.DMA((DOWN_PARTS,)),
-            pltpu.SemaphoreType.DMA((DOWN_PARTS,)),
-            pltpu.SemaphoreType.DMA((3,)),
+            pltpu.SemaphoreType.DMA((parts,)),
+            pltpu.SemaphoreType.DMA((parts,)),
+            pltpu.SemaphoreType.DMA((4,)),
         ],
         compiler_params=pltpu.CompilerParams(
             collective_id=0, has_side_effects=True, vmem_limit_bytes=60 * 1024 * 1024
@@ -753,7 +778,7 @@
         share = tokens.shape[1] // n
         aligned = share == 128 and n & (n - 1) == 0 and n % 4 == 0
         halves = (FF // w_gate.shape[1]) % 2 == 0 and arrays[13].shape[1] == share
-        if aligned and halves and w_gate.shape[1] % COLUMNS == 0 and tokens.shape[0] * n % 64 == 0:
+        if aligned and halves and w_gate.shape[1] % COLUMNS == 0 and tokens.shape[0] * n % 64 == 0 and tokens.shape[1] == sum(DOWN_WIDTHS):
             return local(n, *arrays)
         return plain(*arrays)
 

time: 33.6 us -> 33.3 us (level)
  no operation moved by 1% of the time
where the time goes in v3:
time: 33.3 us; the launch traced here: 33.1 us
  Pallas kernels  32.5 us (98%)
  between operations  0.65 us (2%)
    pallas_call x1, Pallas kernels, local(): pl.pallas_call(functools.partial(fused, n), out_shape=tuple((pltpu.VMEM(s...  31.8 us

profile of v3, /device:TPU:0, one launch (start us, length us, event | category | flops | bytes accessed | tf_op | source)
XLA Modules:
  0.0 33.1 jit_solution(13515031330315982782)
XLA Ops:
  0.6 31.8 %shard_map.193 = (bf16[4,2048]{1,0:T(4,128)(2,1)S(1)}, bf16[4,256]{1,0:T(4,128)(2,1)S(1)}, bf16[4,256]{1,0:T(4,128)(2,1)S(1)}) custom-call(bf16[4,2048]{1,0:T(4,128)(2,1)} %tokens_hbm.1, s32[1,4]{1,0:T(1,128)} %bitcast.12, bf16[4,1024,256]{2,1,0:T(8,128)(2,1)} %ck_hbm.1, bf16[4,1024,256]{2,1,0:T(8,128)(2,1)} %cv_hbm.1, s32[2,4]{1,0:T(2,128)} %bitcast.10, ...), custom_call_target="tpu_custom_call" | custom-call | flops 1409286144 | bytes 22020096 | tf_op jit(solution)/shard_map/pallas_call | solution.py:683
  32.5 0.6 %shard_map.194 = (bf16[4,2048]{1,0:T(4,128)(2,1)}, bf16[4,256]{1,0:T(4,128)(2,1)}, bf16[4,256]{1,0:T(4,128)(2,1)}) custom-call(bf16[4,2048]{1,0:T(4,128)(2,1)S(1)} %get-tuple-element.6.refs_0_, bf16[4,256]{1,0:T(4,128)(2,1)S(1)} %get-tuple-element.7.refs_1_, bf16[4,256]{1,0:T(4,128)(2,1)S(1)} %get-tuple-element.8.refs_2_), custom_call_target="tpu_custom_call" | custom-call | tf_op jit(solution)/shard_map/pallas_call | solution.py:764

commit v4 on v3

--- a/solution.py
+++ b/solution.py
@@ -120,7 +120,7 @@
 WEIGHT_PARTS = 2
 PAIR_LAG = 2
 DOWN_WIDTHS = (512, 512, 512, 512)
-SCHEDULE = (0, (0,), 1, 2, 3, 4, (1,), 5, (2,), 6, (3,), 7, (4,), (5, 6), (7,))
+SCHEDULE = (0, (0,), 1, 2, 3, 4, (1,), 5, (2,), 6, (3,), 7, (4,), (5,), (6,), (7,))
 COLUMNS = 256
 
 

time: 33.3 us -> 33 us (level)
  no operation moved by 1% of the time
where the time goes in v4:
time: 33 us; the launch traced here: 32.9 us
  Pallas kernels  32.2 us (98%)
  between operations  0.65 us (2%)
    pallas_call x1, Pallas kernels, local(): pl.pallas_call(functools.partial(fused, n), out_shape=tuple((pltpu.VMEM(s...  31.6 us

profile of v4, /device:TPU:0, one launch (start us, length us, event | category | flops | bytes accessed | tf_op | source)
XLA Modules:
  0.0 32.9 jit_solution(6364728167494595382)
XLA Ops:
  0.6 31.6 %shard_map.193 = (bf16[4,2048]{1,0:T(4,128)(2,1)S(1)}, bf16[4,256]{1,0:T(4,128)(2,1)S(1)}, bf16[4,256]{1,0:T(4,128)(2,1)S(1)}) custom-call(bf16[4,2048]{1,0:T(4,128)(2,1)} %tokens_hbm.1, s32[1,4]{1,0:T(1,128)} %bitcast.12, bf16[4,1024,256]{2,1,0:T(8,128)(2,1)} %ck_hbm.1, bf16[4,1024,256]{2,1,0:T(8,128)(2,1)} %cv_hbm.1, s32[2,4]{1,0:T(2,128)} %bitcast.10, ...), custom_call_target="tpu_custom_call" | custom-call | flops 1409286144 | bytes 22020096 | tf_op jit(solution)/shard_map/pallas_call | solution.py:683
  32.2 0.6 %shard_map.194 = (bf16[4,2048]{1,0:T(4,128)(2,1)}, bf16[4,256]{1,0:T(4,128)(2,1)}, bf16[4,256]{1,0:T(4,128)(2,1)}) custom-call(bf16[4,2048]{1,0:T(4,128)(2,1)S(1)} %get-tuple-element.6.refs_0_, bf16[4,256]{1,0:T(4,128)(2,1)S(1)} %get-tuple-element.7.refs_1_, bf16[4,256]{1,0:T(4,128)(2,1)S(1)} %get-tuple-element.8.refs_2_), custom_call_target="tpu_custom_call" | custom-call | tf_op jit(solution)/shard_map/pallas_call | solution.py:764
